TPU v7x, 32 devices: a whole 2x2x4 slice. The times are simulated.
32 devices in a mesh: ep: 16 (over z, y, x), tp: 2 (over core).
Axes of the slice: x: 2, y: 2, z: 4, core: 2. Of those that a mesh axis runs over, the one named last changes fastest.
Arguments:
- tokens: bfloat16 [256, 2048], P('ep'), may hold values from -6 to 6
- mix_gain: float32 [2048], replicated, may hold values from 0.1 to 1.9
- query_weight: bfloat16 [2048, 1024], P('ep', 'tp'), may hold values from -0.125 to 0.125
- forget_weight: bfloat16 [2048, 1024], P('ep', 'tp'), may hold values from -0.125 to 0.125
- input_weight: bfloat16 [2048, 1024], P('ep', 'tp'), may hold values from -0.125 to 0.125
- lower_bound: float32 [1024], P('tp'), may hold values from 0 to 0.9
- head_gain: float32 [1024], P('tp'), may hold values from 0.1 to 1.9
- out_weight: bfloat16 [1024, 2048], P('tp', 'ep'), may hold values from -0.1875 to 0.1875
- state: float32 [256, 8, 128, 128], P('ep', 'tp'), may hold values from -4 to 4
- ffn_gain: float32 [2048], replicated, may hold values from 0.1 to 1.9
- route_ids: int32 [256, 2], P('ep'), may hold values from 0 to 7, all different within a row; in each aligned block of 16 rows (0 to 15, 16 to 31, ...) at most 6 rows name the same one
- route_weights: float32 [256, 2], P('ep'), may hold values from 0.25 to 1
- expert_gate: bfloat16 [16, 2048, 2048], P('ep', None, 'tp'), may hold values from -0.125 to 0.125
- expert_up: bfloat16 [16, 2048, 2048], P('ep', None, 'tp'), may hold values from -0.125 to 0.125
- expert_down: bfloat16 [16, 2048, 2048], P('ep', 'tp'), may hold values from -0.09375 to 0.09375
Outputs:
- mixed_out: bfloat16 [256, 2048], P('ep', 'tp')
- new_state: float32 [256, 8, 128, 128], P('ep', 'tp')
Inputs may be any that keep to these rules, and one draw needn't show every extreme that they name: `route_ids`: each row names 2 different experts; among the rows of one device no expert is named by more than 6 rows, a bound that some block reaches of them.
All inputs are finite; a program needn't handle non-finite values.
Results may differ from a plain program's by a relative error of at most 0.015.
Values may be sent and summed in bfloat16 or wider, within the bound.
No kernel may reach another device: no remote copies, remote signals or barrier semaphores. Data moves between devices by JAX's collectives and lax.ppermute only.
A program may use at most 64 MiB of HBM per device.

v0:
```python
import jax
import jax.numpy as jnp
from jax import lax
from jax.sharding import PartitionSpec as P

EXPERTS = 8
TOP = 2


epsilon = 1e-06


def rms_scale(values_in, gain_vec):
    return (
        values_in
        * lax.rsqrt(jnp.mean(values_in * values_in, axis=-1, keepdims=True) + epsilon)
        * gain_vec
    )


def slot_ranks(block_ids, expert_count):
    onehot = (block_ids[..., None] == jnp.arange(expert_count, dtype=jnp.int32)).astype(jnp.int32)
    before = jnp.cumsum(onehot, axis=1) - onehot
    return jnp.sum(before * onehot, axis=-1)


def shards(
    tokens,
    mix_gain,
    query_weight,
    forget_weight,
    input_weight,
    lower_bound,
    head_gain,
    out_weight,
    state,
    ffn_gain,
    route_ids,
    route_weights,
    expert_gate,
    expert_up,
    expert_down,
):
    seq_dev = tokens.shape[0]
    model_width = tokens.shape[1]
    ep_count = lax.axis_size("ep")
    residual = tokens.astype(jnp.float32)
    normed = rms_scale(residual, mix_gain).astype(jnp.bfloat16)
    head_count = state.shape[1]
    head_size = state.shape[2]
    proj_width = query_weight.shape[1]
    pieces = (
        lax.all_gather(query_weight, "ep", axis=0, tiled=True),
        lax.all_gather(forget_weight, "ep", axis=0, tiled=True),
        lax.all_gather(input_weight, "ep", axis=0, tiled=True),
    )
    queries, forget_pre, fresh_values = tuple(
        (jnp.dot(normed, weight_rows, preferred_element_type=jnp.float32) for weight_rows in pieces)
    )
    forget = (lower_bound + (1.0 - lower_bound) * jax.nn.sigmoid(forget_pre)).reshape(
        seq_dev, head_count, head_size
    )
    queries = queries.reshape(seq_dev, head_count, head_size)
    fresh_values = fresh_values.reshape(seq_dev, head_count, head_size)
    new_state = forget[..., None] * state + (1.0 - forget)[..., None] * fresh_values[:, :, None, :]
    readout = jnp.einsum("shk,shkv->shv", queries, new_state, precision=lax.Precision.HIGHEST)
    readout = rms_scale(readout, head_gain.reshape(head_count, head_size))
    heads_out = readout.reshape(seq_dev, proj_width).astype(jnp.bfloat16)
    partial_mix = jnp.dot(
        heads_out,
        lax.all_gather(out_weight, "ep", axis=1, tiled=True),
        preferred_element_type=jnp.float32,
    )
    mixer_sum = lax.psum(partial_mix.astype(jnp.bfloat16), "tp").astype(jnp.float32)
    after_mixer = (residual + mixer_sum).astype(jnp.bfloat16)
    ffn_in = rms_scale(after_mixer.astype(jnp.float32), ffn_gain).astype(jnp.bfloat16)
    capacity = 3 * seq_dev // 8
    expert_span = ep_count // EXPERTS
    half_width = model_width // lax.axis_size("tp")
    own_columns = lax.dynamic_slice_in_dim(
        after_mixer, lax.axis_index("tp") * half_width, half_width, 1
    ).astype(jnp.float32)
    gate_slice = expert_gate[0]
    up_slice = expert_up[0]
    down_slice = expert_down[0]
    slot_iota = jnp.arange(capacity, dtype=jnp.int32)
    own_rank = slot_ranks(route_ids.reshape(1, seq_dev * TOP), EXPERTS).reshape(seq_dev, TOP)
    expert_iota = jnp.arange(EXPERTS, dtype=jnp.int32)
    chosen = (route_ids[:, :, None, None] == expert_iota[None, None, :, None]) & (
        own_rank[:, :, None, None] == slot_iota[None, None, None, :]
    )
    dispatch = jnp.any(chosen, axis=1).astype(jnp.bfloat16)
    combine = jnp.sum(chosen.astype(jnp.float32) * route_weights[:, :, None, None], axis=1)
    outgoing = jnp.einsum(
        "tec,td->ecd", dispatch, ffn_in, preferred_element_type=jnp.float32
    ).astype(jnp.bfloat16)
    outgoing = jnp.broadcast_to(
        outgoing[:, None], (EXPERTS, expert_span, capacity, model_width)
    ).reshape(ep_count, capacity, model_width)
    slot_rows = lax.all_to_all(outgoing, "ep", split_axis=0, concat_axis=0, tiled=True)
    gate_pre = jnp.einsum(
        "...d,df->...f", slot_rows, gate_slice, preferred_element_type=jnp.float32
    )
    up_pre = jnp.einsum("...d,df->...f", slot_rows, up_slice, preferred_element_type=jnp.float32)
    hidden = (jax.nn.silu(gate_pre) * up_pre).astype(jnp.bfloat16)
    partial_out = jnp.einsum(
        "...f,fd->...d", hidden, down_slice, preferred_element_type=jnp.float32
    )
    reduced = lax.psum_scatter(
        partial_out.astype(jnp.bfloat16), "tp", scatter_dimension=2, tiled=True
    ).astype(jnp.float32)
    returned = lax.all_to_all(
        reduced.astype(jnp.bfloat16), "ep", split_axis=0, concat_axis=0, tiled=True
    ).astype(reduced.dtype)
    expert_out = jnp.sum(returned.reshape(EXPERTS, expert_span, capacity, half_width), axis=1)
    expert_mix = jnp.einsum("tec,ecd->td", combine, expert_out, precision=lax.Precision.HIGHEST)
    mixed_out = (own_columns + expert_mix).astype(jnp.bfloat16)
    return (mixed_out, new_state)


def solution(mesh):
    return jax.shard_map(
        shards,
        mesh=mesh,
        in_specs=(
            P("ep", None),
            P(),
            P("ep", "tp"),
            P("ep", "tp"),
            P("ep", "tp"),
            P("tp"),
            P("tp"),
            P("tp", "ep"),
            P("ep", "tp", None, None),
            P(),
            P("ep", None),
            P("ep", None),
            P("ep", None, "tp"),
            P("ep", None, "tp"),
            P("ep", "tp", None),
        ),
        out_specs=(P("ep", "tp"), P("ep", "tp", None, None)),
        check_vma=False,
    )
```

profile of v0, /device:TPU:0, one launch (start us, length us, event | category | flops | bytes accessed | tf_op | source)
XLA Modules:
  0.0 346.5 jit_solution(2052995556414389581)
XLA Ops:
  7.2 0.0 copy-start.1
  7.2 0.0 copy-start.2
  7.2 0.0 all-gather.7.cloned.1.call-start
  7.2 0.7 all-gather.7.cloned.1.call-update
  7.9 0.0 all-gather.9.cloned.1.call-start
  8.0 0.7 all-gather.9.cloned.1.call-update
  8.7 0.0 all-gather.5.cloned.1.call-start
  8.7 0.7 all-gather.5.cloned.1.call-update
  9.4 0.0 all-gather.11.cloned.1.call-start
  9.5 0.5 all-gather.11.cloned.1.call-update
  10.0 0.0 all-reduce.2.cloned.1.call-start
  10.0 0.8 copy.47
  10.8 0.1 eq.68
  10.9 0.1 fusion.48
  10.9 0.1 reduce_window_sum.11
  11.0 0.2 select_reduce_fusion
  11.2 0.1 eq.72
  11.3 0.1 copy.48
  11.4 1.0 fusion.37
  12.4 0.7 iota_compare_fusion.2
  13.1 0.7 broadcast_subtract_fusion.1
  13.7 60.2 %all-gather.7.cloned.1.call-done = bf16[2048,512]{1,0:T(8,128)(2,1)} async-done(((bf16[128,512]{1,0:T(8,128)(2,1)}), bf16[2048,512]{1,0:T(8,128)(2,1)}) %all-gather.7.cloned.1.call-update) | async-done | bytes 2097168 | tf_op jit(solution)/shard_map/all_gather | solution.py:54
  73.9 2.1 fusion.21
  76.0 59.9 %all-gather.9.cloned.1.call-done = bf16[2048,512]{1,0:T(8,128)(2,1)} async-done(((bf16[128,512]{1,0:T(8,128)(2,1)}), bf16[2048,512]{1,0:T(8,128)(2,1)}) %all-gather.9.cloned.1.call-update) | async-done | bytes 2097168 | tf_op jit(solution)/shard_map/all_gather | solution.py:55
  135.9 2.1 fusion.50
  138.0 59.9 %all-gather.5.cloned.1.call-done = bf16[2048,512]{1,0:T(8,128)(2,1)} async-done(((bf16[128,512]{1,0:T(8,128)(2,1)}), bf16[2048,512]{1,0:T(8,128)(2,1)}) %all-gather.5.cloned.1.call-update) | async-done | bytes 2097168 | tf_op jit(solution)/shard_map/all_gather | solution.py:53
  197.9 0.0 copy-done.1
  197.9 0.0 copy-done.2
  197.9 2.0 fusion.53
  199.9 4.4 %multiply_add_fusion = f32[16,4,128,128]{3,2,1,0:T(8,128)S(1)} fusion(f32[16,4,128,128]{3,2,1,0:T(8,128)} %param.23, f32[16,4,128]{2,1,0:T(4,128)S(1)} %mul.124, f32[16,4,128]{2,1,0:T(4,128)S(1)} %broadcast_subtract_fusion, f32[16,4,128]{2,1,0:T(4,128)S(1)} %mul.120), kind=kLoop, calls=%fused_computation.6 | loop fusion | flops 3145728 | bytes 8486912 | tf_op jit(solution)/shard_map/add | solution.py:65
  204.3 0.0 copy-start
  204.3 0.0 copy-start.4
  204.4 0.0 copy-start.3
  204.4 2.0 copy-done
  206.3 3.7 %fusion.56 = f32[16,4,1,128]{3,2,1,0:T(1,128)S(1)} fusion(f32[16,4,128,1]{2,3,1,0:T(1,128)S(1)} %bitcast.52, f32[16,4,128,128]{3,2,1,0:T(8,128)S(1)} %multiply_add_fusion), kind=kOutput, calls=%fused_computation.66 | convolution fusion | flops 12582912 | bytes 4259840 | tf_op jit(solution)/shard_map/shk,shkv->shv/dot_general | solution.py:66
  210.0 0.1 multiply_reduce_fusion
  210.1 0.0 copy-done.4
  210.1 0.1 multiply_convert_fusion
  210.2 52.0 %all-gather.11.cloned.1.call-done = bf16[512,2048]{1,0:T(8,128)(2,1)} async-done(((bf16[512,128]{1,0:T(8,128)(2,1)}), bf16[512,2048]{1,0:T(8,128)(2,1)}) %all-gather.11.cloned.1.call-update) | async-done | bytes 2097168 | tf_op jit(solution)/shard_map/all_gather | solution.py:71
  262.2 2.6 convolution_convert_fusion.1
  264.8 0.0 all-reduce.2.cloned.1.call-update
  264.8 0.0 reduce-scatter.2.cloned.1.call-start
  264.9 16.0 %all-reduce.2.cloned.1.call-done = bf16[16,2048]{1,0:T(8,128)(2,1)} async-done(((bf16[16,2048]{1,0:T(8,128)(2,1)}), bf16[16,2048]{1,0:T(8,128)(2,1)}) %all-reduce.2.cloned.1.call-update) | async-done | bytes 65552 | tf_op jit(solution)/shard_map/psum | solution.py:74
  280.9 1.0 fusion.34
  281.9 0.0 copy-done.3
  281.9 0.3 convolution_convert_fusion
  282.1 0.1 copy.49
  282.3 22.1 %all_to_all.10 = bf16[16,6,2048]{2,1,0:T(8,128)(2,1)S(1)} all-to-all(bf16[16,6,2048]{2,1,0:T(8,128)(2,1)S(1)} %bitcast.49), channel_id=1, replica_groups=mesh['ep'=16,'tp'=2] {'ep'}, dimensions={0} | all-to-all | bytes 786432 | tf_op jit(solution)/shard_map/all_to_all | solution.py:100
  304.4 3.1 fusion.4
  307.5 0.0 copy-start.5
  307.5 5.9 %fusion.6 = bf16[16,6,2048]{2,0,1:T(8,128)(2,1)} fusion(bf16[1,1024,2048]{2,1,0:T(8,128)(2,1)} %param.29, bf16[1,2048,1024]{2,1,0:T(8,128)(2,1)} %param.28, f32[16,6,1024]{2,0,1:T(8,128)S(1)} %fusion.4, bf16[16,6,2048]{2,1,0:T(8,128)(2,1)S(1)} %all_to_all.10), kind=kOutput, calls=%fused_computation.7 | convolution fusion | flops 806092800 | bytes 9568256 | tf_op jit(solution)/shard_map/...f,fd->...d/dot_general | solution.py:106
  313.4 0.0 reduce-scatter.2.cloned.1.call-update
  313.4 6.3 %reduce-scatter.2.cloned.1.call-done = bf16[16,6,1024]{2,0,1:T(8,128)(2,1)} async-done(((bf16[16,6,2048]{2,0,1:T(8,128)(2,1)}), bf16[16,6,1024]{2,0,1:T(8,128)(2,1)}) %reduce-scatter.2.cloned.1.call-update) | async-done | bytes 196624 | tf_op jit(solution)/shard_map/reduce_scatter | solution.py:109
  319.8 1.7 copy.52
  321.5 6.7 %all-to-all-start.1 = ((bf16[16,6,1024]{2,1,0:T(8,128)(2,1)}), bf16[16,6,1024]{2,1,0:T(8,128)(2,1)S(1)}, u32[]{:S(2)}, u32[]{:S(2)}) async-start(bf16[16,6,1024]{2,1,0:T(8,128)(2,1)} %copy.52), calls=%async_computation.2 | async-start | bytes 524288 | tf_op jit(solution)/shard_map/all_to_all | solution.py:112
  328.3 0.0 copy-done.5
  328.3 10.4 %all-to-all-done.1 = bf16[16,6,1024]{2,1,0:T(8,128)(2,1)S(1)} async-done(((bf16[16,6,1024]{2,1,0:T(8,128)(2,1)}), bf16[16,6,1024]{2,1,0:T(8,128)(2,1)S(1)}, u32[]{:S(2)}, u32[]{:S(2)}) %all-to-all-start.1) | async-done | bytes 196640 | tf_op jit(solution)/shard_map/all_to_all | solution.py:112
  338.7 0.1 convert_reduce_fusion
  338.7 0.9 fusion.16
  (11 shorter events, 0.2 us)
Async XLA Ops:
  7.2 190.7 %copy-start.1 = (bf16[16,2048]{1,0:T(8,128)(2,1)S(1)}, bf16[16,2048]{1,0:T(8,128)(2,1)}, u32[]{:S(2)}) copy-start(bf16[16,2048]{1,0:T(8,128)(2,1)} %param.15) | copy-start | bytes 196612
  7.2 190.7 %copy-start.2 = (f32[2048]{0:T(1024)S(1)}, f32[2048]{0:T(1024)}, u32[]{:S(2)}) copy-start(f32[2048]{0:T(1024)} %param.16) | copy-start | bytes 24580
  7.2 66.7 %all-gather.7.cloned.1.call-start = ((), (), s32[]{:S(2)}) async-start(), calls=%async_computation.4 | async-start | bytes 2228224 | tf_op jit(solution)/shard_map/all_gather | solution.py:54
  7.9 128.0 %all-gather.9.cloned.1.call-start = ((), (), s32[]{:S(2)}) async-start(), calls=%async_computation.5 | async-start | bytes 2228224 | tf_op jit(solution)/shard_map/all_gather | solution.py:55
  8.7 189.2 %all-gather.5.cloned.1.call-start = ((), (), s32[]{:S(2)}) async-start(), calls=%async_computation.3 | async-start | bytes 2228224 | tf_op jit(solution)/shard_map/all_gather | solution.py:53
  9.4 252.8 %all-gather.11.cloned.1.call-start = ((), (), s32[]{:S(2)}) async-start(), calls=%async_computation.6 | async-start | bytes 2228224 | tf_op jit(solution)/shard_map/all_gather | solution.py:71
  10.0 270.9 %all-reduce.2.cloned.1.call-start = ((), (), s32[]{:S(2)}) async-start(), calls=%async_computation.7 | async-start | bytes 131072 | tf_op jit(solution)/shard_map/psum | solution.py:74
  204.3 2.0 copy-start
  204.3 5.8 %copy-start.4 = (f32[512]{0:T(512)S(1)}, f32[512]{0:T(512)}, u32[]{:S(2)}) copy-start(f32[512]{0:T(512)} %param.21) | copy-start | bytes 6148
  204.4 77.5 %copy-start.3 = (f32[2048]{0:T(1024)S(1)}, f32[2048]{0:T(1024)}, u32[]{:S(2)}) copy-start(f32[2048]{0:T(1024)} %param.24) | copy-start | bytes 24580
  264.8 55.0 %reduce-scatter.2.cloned.1.call-start = ((), (), s32[]{:S(2)}) async-start(), calls=%async_computation.8 | async-start | bytes 589824 | tf_op jit(solution)/shard_map/reduce_scatter | solution.py:109
  307.5 20.7 %copy-start.5 = (f32[16,2]{0,1:T(2,128)S(1)}, f32[16,2]{0,1:T(2,128)}, u32[]{:S(2)}) copy-start(f32[16,2]{0,1:T(2,128)} %param.26) | copy-start | bytes 388
  321.5 17.1 %all-to-all-start.1 = ((bf16[16,6,1024]{2,1,0:T(8,128)(2,1)}), bf16[16,6,1024]{2,1,0:T(8,128)(2,1)S(1)}, u32[]{:S(2)}, u32[]{:S(2)}) async-start(bf16[16,6,1024]{2,1,0:T(8,128)(2,1)} %copy.52), calls=%async_computation.2 | async-start | bytes 524288 | tf_op jit(solution)/shard_map/all_to_all | solution.py:112
Sparse Core Ops, SparseCore 0:
  10.8 63.0 all-gather.6
  76.7 59.1 all-gather.8
  138.7 59.1 all-gather.4
  200.4 61.7 all-gather.10
  264.9 15.8 all-reduce.1
  313.6 6.1 reduce-scatter.1
where the time goes:
time: 347 us; the launch traced here: 346 us
  waiting for transfers between devices  267 us (77%)
  matrix products  22.6 us (7%)
  blocking collectives  22.1 us (6%)
  between operations  14.3 us (4%)
  other arithmetic  8.35 us (2%)
  starting transfers between devices  6.96 us (2%)
  local copies, waits for them, and re-layouts  4.97 us (1%)
    all_gather x1, waiting for transfers between devices, shards(): lax.all_gather(forget_weight, 'ep', axis=0, tiled=True)  60.2 us
    all_gather x1, waiting for transfers between devices, shards(): lax.all_gather(query_weight, 'ep', axis=0, tiled=True)  59.9 us
    all_gather x1, waiting for transfers between devices, shards(): lax.all_gather(input_weight, 'ep', axis=0, tiled=True)  59.9 us
    all_gather x1, waiting for transfers between devices, shards(): lax.all_gather(out_weight, 'ep', axis=1, tiled=True)  52 us
    all_to_all x1, blocking collectives, shards(): lax.all_to_all(outgoing, 'ep', split_axis=0, concat_axis=0, tiled=True)  22.1 us
    psum x1, waiting for transfers between devices, shards(): lax.psum(partial_mix.astype(jnp.bfloat16), 'tp').astype(jnp.float32)  16 us
    all_to_all x1, waiting for transfers between devices, shards(): lax.all_to_all(reduced.astype(jnp.bfloat16), 'ep', split_axis=0, concat_a...  10.4 us
  transfers between devices with their start and end apart: 7, of which 7 were waited for; matrix products, arithmetic and copies ran while one was open for 5% of the time, Pallas kernels for 0%

commit v1 on v0

--- a/solution.py
+++ b/solution.py
@@ -1,13 +1,355 @@
+import functools
+
 import jax
 import jax.numpy as jnp
 from jax import lax
+from jax.experimental import pallas as pl
+from jax.experimental.pallas import tpu as pltpu
 from jax.sharding import PartitionSpec as P
+
 
 EXPERTS = 8
 TOP = 2
+LANES = 128
+SLOTS = 8
 
 
 epsilon = 1e-06
+
+NEAR = (0, 1, 2, 4)
+GROUP = 4
+
+
+def xor_pairs(count, mask):
+    return [(i, i ^ mask) for i in range(count)]
+
+
+def aligned(start, size):
+    return pl.ds(pl.multiple_of(start, size), size)
+
+
+def call(kernel, args, outs, scratch=(), flops=3_000_000_000, traffic=100_000, mib=4, hbm=False):
+    vmem = pl.BlockSpec(memory_space=pltpu.VMEM)
+    return pl.pallas_call(
+        kernel,
+        out_shape=outs,
+        in_specs=[pl.BlockSpec(memory_space=pltpu.HBM) if hbm else vmem] * len(args),
+        out_specs=[vmem] * len(outs) if isinstance(outs, list) else vmem,
+        scratch_shapes=list(scratch),
+        compiler_params=pltpu.CompilerParams(vmem_limit_bytes=mib << 20),
+        cost_estimate=pl.CostEstimate(flops=flops, bytes_accessed=traffic, transcendentals=0),
+    )(*args)
+
+
+def prep_kernel(coset, tokens_ref, *refs):
+    weight_refs, packed_ref, outs, sems = refs[:3], refs[3], refs[4:-1], refs[-1]
+    me = lax.axis_index("ep")
+    copies = []
+
+    def start(source, target):
+        copy = pltpu.make_async_copy(source, target, sems.at[len(copies)])
+        copy.start()
+        copies.append(copy)
+
+    for k, ref in enumerate(weight_refs):
+        size = ref.shape[1]
+        start(ref, packed_ref.at[:, k * size : (k + 1) * size])
+    for mask, out in zip(coset, outs):
+        for k, near in enumerate(NEAR):
+            block = me ^ (mask ^ near)
+            start(
+                tokens_ref.at[:, aligned(block * LANES, LANES)],
+                out.at[:, k * LANES : (k + 1) * LANES],
+            )
+    for copy in copies:
+        copy.wait()
+
+
+def project_kernel(group, *refs):
+    token_refs, gain_ref, weight_refs, outs = (
+        refs[:group],
+        refs[group],
+        refs[group + 1 : group + 5],
+        refs[group + 5 :],
+    )
+    me = lax.axis_index("ep")
+    rows = jnp.concatenate([ref[...] for ref in token_refs], axis=0)
+    total = None
+    for k, near in enumerate(NEAR):
+        block = me ^ near
+        gain = gain_ref[:, aligned(block * LANES, LANES)]
+        scaled = (rows[:, k * LANES : (k + 1) * LANES].astype(jnp.float32) * gain).astype(jnp.bfloat16)
+        term = jnp.dot(scaled, weight_refs[k][...], preferred_element_type=jnp.float32)
+        total = term if total is None else total + term
+    count = token_refs[0].shape[0]
+    for m, out in enumerate(outs):
+        out[...] = total[m * count : (m + 1) * count].astype(out.dtype)
+
+
+def state_kernel(group, outer, *refs):
+    part_refs = refs[:group]
+    tokens_ref, bound_ref, gain_ref, info_ref, state_ref = refs[group : group + 5]
+    new_ref = refs[group + 5]
+    payloads = refs[group + 6 :]
+    count = tokens_ref.shape[0]
+    proj = bound_ref.shape[1]
+    half = outer // 2
+
+    tokens = tokens_ref[...].astype(jnp.float32)
+    scale = lax.rsqrt(jnp.mean(tokens * tokens, axis=-1, keepdims=True) + epsilon)
+    for head in range(proj // LANES):
+
+        def pick(which):
+            at = slice(which * proj + head * LANES, which * proj + (head + 1) * LANES)
+            total = part_refs[0][:, at].astype(jnp.float32)
+            for ref in part_refs[1:]:
+                total = total + ref[:, at].astype(jnp.float32)
+            return total * scale
+
+        cols = slice(head * LANES, (head + 1) * LANES)
+        bound = bound_ref[:, cols]
+        forget = bound + (1.0 - bound) * jax.nn.sigmoid(pick(0))
+        fresh = pick(1)
+        query = pick(2)
+        forget_t = forget.T
+        query_t = query.T
+        rows = []
+        for s in range(count):
+            row = fresh[s : s + 1, :]
+            new = row + forget_t[:, s : s + 1] * (state_ref[s, head] - row)
+            new_ref[s, head] = new
+            rows.append(jnp.sum(query_t[:, s : s + 1] * new, axis=0, keepdims=True))
+        readout = jnp.concatenate(rows, axis=0)
+        normed = (
+            readout
+            * lax.rsqrt(jnp.mean(readout * readout, axis=-1, keepdims=True) + epsilon)
+            * gain_ref[:, cols]
+        ).astype(jnp.bfloat16)
+        for out in payloads:
+            out[:, cols] = normed
+
+    core = lax.axis_index("tp")
+    place = lax.axis_index("ep") % GROUP
+    for m, out in enumerate(payloads):
+        for a in range(half):
+            block = (core * half + a) * GROUP + (place ^ m)
+            out[:, proj + a * LANES : proj + (a + 1) * LANES] = tokens_ref[:, aligned(block * LANES, LANES)]
+        out[:, proj + half * LANES :] = info_ref[...]
+
+
+def mix_kernel(outer, *refs):
+    payloads = refs[:GROUP]
+    weights = refs[GROUP : GROUP + outer]
+    own_ref, other_ref, resid_ref, info_ref, heads_ref, part_ref = refs[GROUP + outer :]
+    me = lax.axis_index("ep")
+    core = lax.axis_index("tp")
+    place = me % GROUP
+    line = me // GROUP
+    half = outer // 2
+    count = payloads[0].shape[0]
+    proj = weights[0].shape[0]
+    for m, ref in enumerate(payloads):
+        at = aligned((place ^ m) * count, count)
+        heads_ref[at, :] = ref[:, :proj]
+        resid_ref[at, :] = ref[:, proj : proj + half * LANES]
+        info_ref[at, :] = ref[:, proj + half * LANES :]
+    heads = heads_ref[...]
+    for m, ref in enumerate(weights):
+        product = jnp.dot(heads, ref[...], preferred_element_type=jnp.float32)
+        part_ref[:, aligned((line ^ m) * LANES, LANES)] = product.astype(jnp.bfloat16)
+    size = half * LANES
+    own_ref[...] = part_ref[:, aligned(core * size, size)]
+    other_ref[...] = part_ref[:, aligned((1 - core) * size, size)]
+
+
+def dispatch_kernel(span, own_ref, got_ref, resid_ref, info_ref, out_ref, *rest):
+    backs, after_ref = rest[:-1], rest[-1]
+    mixer = own_ref[...].astype(jnp.float32) + got_ref[...].astype(jnp.float32)
+    after_ref[...] = (resid_ref[...].astype(jnp.float32) + mixer).astype(jnp.bfloat16)
+    place = lax.axis_index("ep") % GROUP
+    count = after_ref.shape[0] // GROUP
+    for m, ref in enumerate(backs):
+        ref[...] = after_ref[aligned((place ^ m) * count, count), :]
+    after = after_ref[...]
+    slots = info_ref[...].astype(jnp.float32).T
+    rows = GROUP * SLOTS
+    row = lax.broadcasted_iota(jnp.int32, (rows, after.shape[0]), 0)
+    col = lax.broadcasted_iota(jnp.int32, (rows, after.shape[0]), 1)
+    same = (row // SLOTS) == (col // count)
+    slot = (row % SLOTS).astype(jnp.float32)
+    for e in range(EXPERTS):
+        chosen = same & (slots[e : e + 1, :] == slot)
+        select = jnp.where(chosen, 1.0, 0.0).astype(jnp.bfloat16)
+        picked = jnp.dot(select, after, preferred_element_type=jnp.float32).astype(jnp.bfloat16)
+        for sp in range(span):
+            out_ref[e * span + sp] = picked
+
+
+def expert_kernel(outer, mine_ref, theirs_ref, gain_ref, gate_ref, up_ref, down_ref, own_ref, other_ref, rows_ref, total_ref):
+    core = lax.axis_index("tp")
+    half = outer // 2
+    width = rows_ref.shape[1] // 2
+    block = GROUP * SLOTS
+    for ref, side in ((mine_ref, core), (theirs_ref, 1 - core)):
+        for z in range(outer):
+            for q in range(GROUP):
+                for a in range(half):
+                    at = side * width + (a * GROUP + q) * LANES
+                    rows_ref[z * block : (z + 1) * block, aligned(at, LANES)] = ref[
+                        z * GROUP + q, :, a * LANES : (a + 1) * LANES
+                    ]
+    values = rows_ref[...].astype(jnp.float32)
+    scale = lax.rsqrt(jnp.mean(values * values, axis=-1, keepdims=True) + epsilon)
+    rows = (values * scale * gain_ref[...]).astype(jnp.bfloat16)
+    gate = jnp.dot(rows, gate_ref[0], preferred_element_type=jnp.float32)
+    up = jnp.dot(rows, up_ref[0], preferred_element_type=jnp.float32)
+    hidden = (jax.nn.silu(gate) * up).astype(jnp.bfloat16)
+    total_ref[...] = jnp.dot(hidden, down_ref[0], preferred_element_type=jnp.float32).astype(jnp.bfloat16)
+    own_ref[...] = total_ref[:, aligned(core * width, width)]
+    other_ref[...] = total_ref[:, aligned((1 - core) * width, width)]
+
+
+def combine_kernel(outer, got_ref, weight_ref, *refs):
+    afters, out_ref, base_ref = refs[:GROUP], refs[GROUP], refs[GROUP + 1]
+    place = lax.axis_index("ep") % GROUP
+    half = outer // 2
+    for m, ref in enumerate(afters):
+        for a in range(half):
+            at = (a * GROUP + (place ^ m)) * LANES
+            base_ref[:, aligned(at, LANES)] = ref[:, a * LANES : (a + 1) * LANES].astype(jnp.float32)
+    weight = weight_ref[...]
+    high = weight.astype(jnp.bfloat16)
+    rest = weight - high.astype(jnp.float32)
+    middle = rest.astype(jnp.bfloat16)
+    low = (rest - middle.astype(jnp.float32)).astype(jnp.bfloat16)
+    values = got_ref[...]
+    mix = jnp.dot(high, values, preferred_element_type=jnp.float32)
+    mix = mix + jnp.dot(middle, values, preferred_element_type=jnp.float32)
+    mix = mix + jnp.dot(low, values, preferred_element_type=jnp.float32)
+    out_ref[...] = (base_ref[...] + mix).astype(jnp.bfloat16)
+
+
+def fast_shards(
+    tokens,
+    mix_gain,
+    query_weight,
+    forget_weight,
+    input_weight,
+    lower_bound,
+    head_gain,
+    out_weight,
+    state,
+    ffn_gain,
+    route_ids,
+    route_weights,
+    expert_gate,
+    expert_up,
+    expert_down,
+):
+    bf16, f32 = jnp.bfloat16, jnp.float32
+    ep = lax.axis_size("ep")
+    count, width = tokens.shape
+    proj = query_weight.shape[1]
+    outer = ep // GROUP
+    half = outer // 2
+    span = ep // EXPERTS
+    coset = [h * 8 + b for h in range(ep // 8) for b in (0, 7)]
+
+    def move(value, mask):
+        if not mask:
+            return value
+        return lax.ppermute(value, "ep", xor_pairs(ep, mask))
+
+    def swap(value):
+        return lax.ppermute(value, "tp", [(0, 1), (1, 0)])
+
+    def shaped(*shape, dtype=bf16):
+        return jax.ShapeDtypeStruct(shape, dtype)
+
+    packed, *sent = call(
+        functools.partial(prep_kernel, coset),
+        [pltpu.with_memory_space_constraint(a, pltpu.HBM) for a in (tokens, forget_weight, input_weight, query_weight)],
+        [shaped(LANES, 3 * proj)] + [shaped(count, len(NEAR) * LANES)] * len(coset),
+        scratch=[pltpu.SemaphoreType.DMA((3 + len(coset) * len(NEAR),))],
+        hbm=True,
+    )
+    weights = [move(packed, near) for near in NEAR]
+    token_blocks = [move(value, mask) for value, mask in zip(sent, coset)]
+    out_weights = [move(out_weight, GROUP * m) for m in range(outer)]
+
+    experts = jnp.arange(EXPERTS, dtype=jnp.int32)
+    named = route_ids[:, :, None] == experts
+    chosen = jnp.any(named, axis=1)
+    before = (jnp.arange(count)[:, None] > jnp.arange(count)[None, :]).astype(f32)
+    rank = jnp.sum(before[:, :, None] * chosen.astype(f32)[None, :, :], axis=1)
+    slot_of = jnp.where(chosen, rank, 2.0 * SLOTS)
+    share = jnp.sum(jnp.where(named, route_weights[:, :, None], 0.0), axis=1)
+    info = jnp.pad(slot_of, ((0, 0), (0, LANES - EXPERTS))).astype(bf16)
+    places = jnp.arange(SLOTS, dtype=jnp.int32).astype(f32)
+    combine = jnp.where(slot_of[:, :, None, None] == places, share[:, :, None, None], 0.0)
+    combine = jnp.broadcast_to(combine, (count, EXPERTS, span, SLOTS)).reshape(count, ep * SLOTS)
+
+    parts = call(
+        functools.partial(project_kernel, len(coset)),
+        (*token_blocks, mix_gain.reshape(1, width), *weights),
+        [shaped(count, 3 * proj)] * len(coset),
+    )
+    parts = [move(value, mask) for value, mask in zip(parts, coset)]
+
+    pay = proj + half * LANES + LANES
+    args = (
+        *parts,
+        tokens,
+        lower_bound.reshape(1, proj),
+        head_gain.reshape(1, proj),
+        info,
+        state,
+    )
+    new_state, *payloads = call(
+        functools.partial(state_kernel, len(coset), outer),
+        args,
+        [shaped(*state.shape, dtype=f32)] + [shaped(count, pay)] * GROUP,
+        mib=14,
+    )
+    payloads = [move(value, m) for m, value in enumerate(payloads)]
+
+    tall = GROUP * count
+    own, other, resid, infos = call(
+        functools.partial(mix_kernel, outer),
+        (*payloads, *out_weights),
+        [shaped(tall, half * LANES)] * 3 + [shaped(tall, LANES)],
+        scratch=[pltpu.VMEM((tall, proj), bf16), pltpu.VMEM((tall, outer * LANES), bf16)],
+    )
+    got = swap(other)
+    outgoing, *afters = call(
+        functools.partial(dispatch_kernel, span),
+        (own, got, resid, infos),
+        [shaped(ep, GROUP * SLOTS, half * LANES)] + [shaped(count, half * LANES)] * GROUP,
+        scratch=[pltpu.VMEM((tall, half * LANES), bf16)],
+    )
+    slot_rows = lax.all_to_all(outgoing, "ep", split_axis=0, concat_axis=0, tiled=True)
+    afters = [move(value, m) for m, value in enumerate(afters)]
+    other_rows = swap(slot_rows)
+
+    total_rows = ep * SLOTS
+    mine, theirs = call(
+        functools.partial(expert_kernel, outer),
+        (slot_rows, other_rows, ffn_gain.reshape(1, width), expert_gate, expert_up, expert_down),
+        [shaped(total_rows, width // 2)] * 2,
+        scratch=[pltpu.VMEM((total_rows, width), bf16), pltpu.VMEM((total_rows, width), bf16)],
+        mib=24,
+    )
+    reduced = (mine.astype(f32) + swap(theirs).astype(f32)).astype(bf16)
+    returned = lax.all_to_all(
+        reduced.reshape(ep, SLOTS, width // 2), "ep", split_axis=0, concat_axis=0, tiled=True
+    )
+    mixed_out = call(
+        functools.partial(combine_kernel, outer),
+        (returned.reshape(total_rows, width // 2), combine, *afters),
+        shaped(count, width // 2),
+        scratch=[pltpu.VMEM((count, width // 2), f32)],
+    )
+    return (mixed_out, new_state)
 
 
 def rms_scale(values_in, gain_vec):
@@ -24,7 +366,7 @@
     return jnp.sum(before * onehot, axis=-1)
 
 
-def shards(
+def general_shards(
     tokens,
     mix_gain,
     query_weight,
@@ -118,6 +460,25 @@
     return (mixed_out, new_state)
 
 
+def shards(*args):
+    tokens, query_weight, state = args[0], args[2], args[8]
+    ep, tp = lax.axis_size("ep"), lax.axis_size("tp")
+    fits = (
+        tp == 2
+        and ep % 8 == 0
+        and ep % EXPERTS == 0
+        and tokens.shape[0] % 16 == 0
+        and 3 * tokens.shape[0] // 8 <= SLOTS
+        and tokens.shape[1] == ep * LANES
+        and query_weight.shape[0] == LANES
+        and state.shape[2:] == (LANES, LANES)
+        and args[12].shape[2] % (4 * LANES) == 0
+    )
+    if not fits:
+        return general_shards(*args)
+    return fast_shards(*args)
+
+
 def solution(mesh):
     return jax.shard_map(
         shards,

time: 347 us -> 86.8 us (0.25)
  waiting for transfers between devices: 267 us -> 26.7 us
  starting transfers between devices: 6.96 us -> 33.2 us
  matrix products: 22.6 us -> 0 us
  between operations: 14.3 us -> 0.84 us
  Pallas kernels: 0 us -> 10.7 us
  blocking collectives: 22.1 us -> 13.7 us
  other arithmetic: 8.35 us -> 0.95 us
  local copies, waits for them, and re-layouts: 4.97 us -> 0.28 us
    all_gather x4 -> x0, waiting for transfers between devices: 232 us -> none  [the longest x1 60.2 us: shards(): lax.all_gather(forget_weight, 'ep', axis=0, tiled=True)]
    ppermute x0 -> x21, starting transfers between devices: none -> 29.7 us  [the longest x18 29.4 us: move(): return lax.ppermute(value, 'ep', xor_pairs(ep, mask))]
    ppermute x0 -> x21, waiting for transfers between devices: none -> 24.4 us  [the longest x18 20.3 us: move(): return lax.ppermute(value, 'ep', xor_pairs(ep, mask))]
    dot_general x9 -> x0, matrix products: 22.6 us -> none  [the longest x3 6.16 us: shards(): jnp.dot(normed, weight_rows, preferred_element_type=jnp.float32)]
    psum x1 -> x0, waiting for transfers between devices: 16 us -> none  [shards(): lax.psum(partial_mix.astype(jnp.bfloat16), 'tp').astype(jnp.float32)]
    pallas_call x0 -> x7, Pallas kernels: none -> 10.7 us  [call(): pl.pallas_call(kernel, out_shape=outs, in_specs=[pl.BlockSpec(memory_spac...]
    all_to_all x1, blocking collectives: 22.1 us -> 13.7 us  [fast_shards(): lax.all_to_all(outgoing, 'ep', split_axis=0, concat_axis=0, tiled=True)]
    all_to_all x1, waiting for transfers between devices: 10.4 us -> 2.3 us  [fast_shards(): lax.all_to_all(reduced.reshape(ep, SLOTS, width // 2), 'ep', split_axis=0...]
  transfers between devices with their start and end apart: 7 -> 22, of which waited for: 7 -> 13; matrix products, arithmetic and copies ran while one was open for 5% -> 0% of each run, Pallas kernels for 0% -> 7%
where the time goes in v1:
time: 86.8 us; the launch traced here: 86.5 us
  starting transfers between devices  33.2 us (38%)
  waiting for transfers between devices  26.7 us (31%)
  blocking collectives  13.7 us (16%)
  Pallas kernels  10.7 us (12%)
  other arithmetic  0.95 us (1%)
    ppermute x18, starting transfers between devices, move(): return lax.ppermute(value, 'ep', xor_pairs(ep, mask))  29.4 us
    ppermute x18, waiting for transfers between devices, move(): return lax.ppermute(value, 'ep', xor_pairs(ep, mask))  20.3 us
    all_to_all x1, blocking collectives, fast_shards(): lax.all_to_all(outgoing, 'ep', split_axis=0, concat_axis=0, tiled=True)  13.7 us
    pallas_call x7, Pallas kernels, call(): pl.pallas_call(kernel, out_shape=outs, in_specs=[pl.BlockSpec(memory_spac...  10.7 us
    ppermute x3, waiting for transfers between devices, swap(): return lax.ppermute(value, 'tp', [(0, 1), (1, 0)])  4.13 us
    all_to_all x1, starting transfers between devices, fast_shards(): lax.all_to_all(reduced.reshape(ep, SLOTS, width // 2), 'ep', split_axis=0...  3.55 us
    all_to_all x1, waiting for transfers between devices, fast_shards(): lax.all_to_all(reduced.reshape(ep, SLOTS, width // 2), 'ep', split_axis=0...  2.3 us
  transfers between devices with their start and end apart: 22, of which 13 were waited for; matrix products, arithmetic and copies ran while one was open for 0% of the time, Pallas kernels for 7%

profile of v1, /device:TPU:0, one launch (start us, length us, event | category | flops | bytes accessed | tf_op | source)
XLA Modules:
  0.0 86.5 jit_solution(15063851884472007928)
XLA Ops:
  0.7 1.3 %shard_map.158 = (bf16[128,1536]{1,0:T(8,128)(2,1)S(1)}, bf16[16,512]{1,0:T(8,128)(2,1)S(1)}, bf16[16,512]{1,0:T(8,128)(2,1)S(1)}, bf16[16,512]{1,0:T(8,128)(2,1)S(1)}, bf16[16,512]{1,0:T(8,128)(2,1)S(1)}) custom-call(bf16[16,2048]{1,0:T(8,128)(2,1)} %refs_4_.2, bf16[128,512]{1,0:T(8,128)(2,1)} %refs_0_.1, bf16[128,512]{1,0:T(8,128)(2,1)} %refs_1_.1, ...), custom_call_target="tpu_custom_call" | custom-call | flops 3000000000 | bytes 100000 | tf_op jit(solution)/shard_map/pallas_call | solution.py:33
  1.9 3.1 %collective-permute-start.5 = (bf16[128,1536]{1,0:T(8,128)(2,1)S(1)}, bf16[128,1536]{1,0:T(8,128)(2,1)S(1)}, u32[]{:S(2)}, u32[]{:S(2)}) collective-permute-start(bf16[128,1536]{1,0:T(8,128)(2,1)S(1)} %get-tuple-element.31.refs_5_), channel_id=1, source_target_pairs={{0,8},{2,10},{4,12},{6,14},{8,0},{10,2},{12,4},{14,6},{16,24},{18,... | collective-permute-start | bytes 1179656 | tf_op jit(solution)/shard_map/ppermute | solution.py:261
  5.1 1.5 %collective-permute-start.4 = (bf16[128,1536]{1,0:T(8,128)(2,1)S(1)}, bf16[128,1536]{1,0:T(8,128)(2,1)S(1)}, u32[]{:S(2)}, u32[]{:S(2)}) collective-permute-start(bf16[128,1536]{1,0:T(8,128)(2,1)S(1)} %get-tuple-element.31.refs_5_), channel_id=1, source_target_pairs={{0,4},{2,6},{4,0},{6,2},{8,12},{10,14},{12,8},{14,10},{16,20},{18,... | collective-permute-start | bytes 1179656 | tf_op jit(solution)/shard_map/ppermute | solution.py:261
  6.6 1.5 %collective-permute-start.3 = (bf16[128,1536]{1,0:T(8,128)(2,1)S(1)}, bf16[128,1536]{1,0:T(8,128)(2,1)S(1)}, u32[]{:S(2)}, u32[]{:S(2)}) collective-permute-start(bf16[128,1536]{1,0:T(8,128)(2,1)S(1)} %get-tuple-element.31.refs_5_), channel_id=1, source_target_pairs={{0,2},{2,0},{4,6},{6,4},{8,10},{10,8},{12,14},{14,12},{16,18},{18,... | collective-permute-start | bytes 1179656 | tf_op jit(solution)/shard_map/ppermute | solution.py:261
  8.1 0.0 collective-permute-start
  8.1 2.9 %collective-permute-start.1 = (bf16[16,512]{1,0:T(8,128)(2,1)S(1)}, bf16[16,512]{1,0:T(8,128)(2,1)S(1)}, u32[]{:S(2)}, u32[]{:S(2)}) collective-permute-start(bf16[16,512]{1,0:T(8,128)(2,1)S(1)} %get-tuple-element.29), channel_id=1, source_target_pairs={{0,16},{2,18},{4,20},{6,22},{8,24},{10,26},{12,28},{14,30},{16,0},... | collective-permute-start | bytes 49160 | tf_op jit(solution)/shard_map/ppermute | solution.py:261
  11.0 6.0 %collective-permute-done.refs_1_ = bf16[16,512]{1,0:T(8,128)(2,1)S(1)} collective-permute-done((bf16[16,512]{1,0:T(8,128)(2,1)S(1)}, bf16[16,512]{1,0:T(8,128)(2,1)S(1)}, u32[]{:S(2)}, u32[]{:S(2)}) %collective-permute-start) | collective-permute-done | bytes 16416 | tf_op jit(solution)/shard_map/ppermute | solution.py:261
  17.0 3.5 %collective-permute-start.2 = (bf16[16,512]{1,0:T(8,128)(2,1)S(1)}, bf16[16,512]{1,0:T(8,128)(2,1)S(1)}, u32[]{:S(2)}, u32[]{:S(2)}) collective-permute-start(bf16[16,512]{1,0:T(8,128)(2,1)S(1)} %get-tuple-element.30), channel_id=1, source_target_pairs={{0,30},{2,28},{4,26},{6,24},{8,22},{10,20},{12,18},{14,16},{16,14}... | collective-permute-start | bytes 49160 | tf_op jit(solution)/shard_map/ppermute | solution.py:261
  20.5 0.1 multiply_reduce_fusion
  20.6 0.1 copy.23
  20.7 0.0 collective-permute-done.1.refs_2_
  20.7 0.1 collective-permute-start.13
  20.8 3.8 %collective-permute-done.2.refs_3_ = bf16[16,512]{1,0:T(8,128)(2,1)S(1)} collective-permute-done((bf16[16,512]{1,0:T(8,128)(2,1)S(1)}, bf16[16,512]{1,0:T(8,128)(2,1)S(1)}, u32[]{:S(2)}, u32[]{:S(2)}) %collective-permute-start.2) | collective-permute-done | bytes 16416 | tf_op jit(solution)/shard_map/ppermute | solution.py:261
  24.6 0.9 %collective-permute-start.12 = (bf16[512,128]{1,0:T(8,128)(2,1)S(1)}, bf16[512,128]{1,0:T(8,128)(2,1)S(1)}, u32[]{:S(2)}, u32[]{:S(2)}) collective-permute-start(bf16[512,128]{1,0:T(8,128)(2,1)S(1)} %copy-done.5), channel_id=1, source_target_pairs={{0,8},{2,10},{4,12},{6,14},{8,0},{10,2},{12,4},{14,6},{16,24},{18,... | collective-permute-start | bytes 393224 | tf_op jit(solution)/shard_map/ppermute | solution.py:261
  25.5 0.0 collective-permute-done.5.refs_8_
  25.5 0.0 collective-permute-done.4.refs_7_
  25.5 0.0 collective-permute-done.3.refs_6_
  25.5 0.0 copy-start.4
  25.5 0.0 copy-start.6
  25.5 0.0 copy-start.8
  25.6 0.0 copy-start.9
  25.6 0.4 shard_map.159
  25.9 1.0 %collective-permute-start.6 = (bf16[16,1536]{1,0:T(8,128)(2,1)S(1)}, bf16[16,1536]{1,0:T(8,128)(2,1)S(1)}, u32[]{:S(2)}, u32[]{:S(2)}) collective-permute-start(bf16[16,1536]{1,0:T(8,128)(2,1)S(1)} %get-tuple-element.33), channel_id=1, source_target_pairs={{0,14},{2,12},{4,10},{6,8},{8,6},{10,4},{12,2},{14,0},{16,30},{18,... | collective-permute-start | bytes 147464 | tf_op jit(solution)/shard_map/ppermute | solution.py:261
  26.9 2.3 %collective-permute-start.7 = (bf16[16,1536]{1,0:T(8,128)(2,1)S(1)}, bf16[16,1536]{1,0:T(8,128)(2,1)S(1)}, u32[]{:S(2)}, u32[]{:S(2)}) collective-permute-start(bf16[16,1536]{1,0:T(8,128)(2,1)S(1)} %get-tuple-element.34), channel_id=1, source_target_pairs={{0,16},{2,18},{4,20},{6,22},{8,24},{10,26},{12,28},{14,30},{16,0},... | collective-permute-start | bytes 147464 | tf_op jit(solution)/shard_map/ppermute | solution.py:261
  29.2 3.2 %collective-permute-start.8 = (bf16[16,1536]{1,0:T(8,128)(2,1)S(1)}, bf16[16,1536]{1,0:T(8,128)(2,1)S(1)}, u32[]{:S(2)}, u32[]{:S(2)}) collective-permute-start(bf16[16,1536]{1,0:T(8,128)(2,1)S(1)} %get-tuple-element.35), channel_id=1, source_target_pairs={{0,30},{2,28},{4,26},{6,24},{8,22},{10,20},{12,18},{14,16},{16,14}... | collective-permute-start | bytes 147464 | tf_op jit(solution)/shard_map/ppermute | solution.py:261
  32.4 0.0 collective-permute-done.6.refs_1_
  32.4 2.4 %collective-permute-start.14 = (bf16[512,128]{1,0:T(8,128)(2,1)S(1)}, bf16[512,128]{1,0:T(8,128)(2,1)S(1)}, u32[]{:S(2)}, u32[]{:S(2)}) collective-permute-start(bf16[512,128]{1,0:T(8,128)(2,1)S(1)} %copy-done.5), channel_id=1, source_target_pairs={{0,24},{2,26},{4,28},{6,30},{8,16},{10,18},{12,20},{14,22},{16,8},... | collective-permute-start | bytes 393224 | tf_op jit(solution)/shard_map/ppermute | solution.py:261
  34.8 0.0 collective-permute-done.7.refs_2_
  34.8 2.2 %collective-permute-done.8.refs_3_ = bf16[16,1536]{1,0:T(8,128)(2,1)S(1)} collective-permute-done((bf16[16,1536]{1,0:T(8,128)(2,1)S(1)}, bf16[16,1536]{1,0:T(8,128)(2,1)S(1)}, u32[]{:S(2)}, u32[]{:S(2)}) %collective-permute-start.8) | collective-permute-done | bytes 49184 | tf_op jit(solution)/shard_map/ppermute | solution.py:261
  37.0 0.0 copy-done.9
  37.0 5.5 %shard_map.160 = (f32[16,4,128,128]{3,2,1,0:T(8,128)}, bf16[16,896]{1,0:T(8,128)(2,1)S(1)}, bf16[16,896]{1,0:T(8,128)(2,1)S(1)}, bf16[16,896]{1,0:T(8,128)(2,1)S(1)}, bf16[16,896]{1,0:T(8,128)(2,1)S(1)}) custom-call(bf16[16,1536]{1,0:T(8,128)(2,1)S(1)} %get-tuple-element.32.refs_0_, bf16[16,1536]{1,0:T(8,128)(2,1)S(1)} %collective-permute-done.6.refs_1_, ...), custom_call_target="tpu_custom_call" | custom-call | flops 3000000000 | bytes 100000 | tf_op jit(solution)/shard_map/pallas_call | solution.py:33
  42.5 1.3 %collective-permute-start.9 = (bf16[16,896]{1,0:T(8,128)(2,1)S(1)}, bf16[16,896]{1,0:T(8,128)(2,1)S(1)}, u32[]{:S(2)}, u32[]{:S(2)}) collective-permute-start(bf16[16,896]{1,0:T(8,128)(2,1)S(1)} %get-tuple-element.37), channel_id=1, source_target_pairs={{0,2},{2,0},{4,6},{6,4},{8,10},{10,8},{12,14},{14,12},{16,18},{18,... | collective-permute-start | bytes 86024 | tf_op jit(solution)/shard_map/ppermute | solution.py:261
  43.9 1.4 %collective-permute-start.10 = (bf16[16,896]{1,0:T(8,128)(2,1)S(1)}, bf16[16,896]{1,0:T(8,128)(2,1)S(1)}, u32[]{:S(2)}, u32[]{:S(2)}) collective-permute-start(bf16[16,896]{1,0:T(8,128)(2,1)S(1)} %get-tuple-element.38), channel_id=1, source_target_pairs={{0,4},{2,6},{4,0},{6,2},{8,12},{10,14},{12,8},{14,10},{16,20},{18,... | collective-permute-start | bytes 86024 | tf_op jit(solution)/shard_map/ppermute | solution.py:261
  45.3 0.0 collective-permute-done.13.refs_6_
  45.3 0.7 collective-permute-start.11
  46.0 0.0 collective-permute-done.12.refs_5_
  46.0 0.0 collective-permute-done.14.refs_7_
  46.0 0.4 collective-permute-done.9.refs_1_
  46.4 1.3 %collective-permute-done.10.refs_2_ = bf16[16,896]{1,0:T(8,128)(2,1)S(1)} collective-permute-done((bf16[16,896]{1,0:T(8,128)(2,1)S(1)}, bf16[16,896]{1,0:T(8,128)(2,1)S(1)}, u32[]{:S(2)}, u32[]{:S(2)}) %collective-permute-start.10) | collective-permute-done | bytes 28704 | tf_op jit(solution)/shard_map/ppermute | solution.py:261
  47.7 2.3 %collective-permute-done.11.refs_3_ = bf16[16,896]{1,0:T(8,128)(2,1)S(1)} collective-permute-done((bf16[16,896]{1,0:T(8,128)(2,1)S(1)}, bf16[16,896]{1,0:T(8,128)(2,1)S(1)}, u32[]{:S(2)}, u32[]{:S(2)}) %collective-permute-start.11) | collective-permute-done | bytes 28704 | tf_op jit(solution)/shard_map/ppermute | solution.py:261
  50.0 0.2 shard_map.161
  50.3 0.1 collective-permute-start.15
  50.4 1.2 %collective-permute-done.15.got_ref = bf16[64,256]{1,0:T(8,128)(2,1)S(1)} collective-permute-done((bf16[64,256]{1,0:T(8,128)(2,1)S(1)}, bf16[64,256]{1,0:T(8,128)(2,1)S(1)}, u32[]{:S(2)}, u32[]{:S(2)}) %collective-permute-start.15) | collective-permute-done | bytes 32800 | tf_op jit(solution)/shard_map/ppermute | solution.py:264
  51.6 0.2 shard_map.162
  51.8 13.7 %all_to_all.10.mine_ref = bf16[16,32,256]{2,1,0:T(8,128)(2,1)S(1)} all-to-all(bf16[16,32,256]{2,1,0:T(8,128)(2,1)S(1)} %get-tuple-element.44), channel_id=1, replica_groups=mesh['ep'=16,'tp'=2] {'ep'}, dimensions={0} | all-to-all | bytes 524288 | tf_op jit(solution)/shard_map/all_to_all | solution.py:330
  65.5 0.0 collective-permute-start.16
  65.5 1.5 %collective-permute-done.16.theirs_ref = bf16[16,32,256]{2,1,0:T(8,128)(2,1)S(1)} collective-permute-done((bf16[16,32,256]{2,1,0:T(8,128)(2,1)S(1)}, bf16[16,32,256]{2,1,0:T(8,128)(2,1)S(1)}, u32[]{:S(2)}, u32[]{:S(2)}) %collective-permute-start.16) | collective-permute-done | bytes 262176 | tf_op jit(solution)/shard_map/ppermute | solution.py:264
  67.1 0.0 copy-start.11
  67.1 2.2 %shard_map.163 = (bf16[128,1024]{1,0:T(8,128)(2,1)S(1)}, bf16[128,1024]{1,0:T(8,128)(2,1)S(1)}) custom-call(bf16[16,32,256]{2,1,0:T(8,128)(2,1)S(1)} %all_to_all.10.mine_ref, bf16[16,32,256]{2,1,0:T(8,128)(2,1)S(1)} %collective-permute-done.16.theirs_ref, f32[1,2048]{1,0:T(1,128)S(1)} %bitcast.9, bf16[1,2048,1024]{2,1,0:T(8,128)(2,1)S(1)} %copy-done, ...), custom_call_target="tpu_custom_call" | custom-call | flops 3000000000 | bytes 100000 | tf_op jit(solution)/shard_map/pallas_call | solution.py:33
  69.3 0.2 collective-permute-start.17
  69.5 1.4 %collective-permute-done.17 = bf16[128,1024]{1,0:T(8,128)(2,1)S(1)} collective-permute-done((bf16[128,1024]{1,0:T(8,128)(2,1)S(1)}, bf16[128,1024]{1,0:T(8,128)(2,1)S(1)}, u32[]{:S(2)}, u32[]{:S(2)}) %collective-permute-start.17) | collective-permute-done | bytes 262176 | tf_op jit(solution)/shard_map/ppermute | solution.py:264
  70.9 0.8 fusion
  71.7 3.5 %all-to-all-start.1 = ((bf16[16,8,1024]{2,1,0:T(8,128)(2,1)}), bf16[16,8,1024]{2,1,0:T(8,128)(2,1)S(1)}, u32[]{:S(2)}, u32[]{:S(2)}) async-start(bf16[16,8,1024]{2,1,0:T(8,128)(2,1)} %fusion), calls=%async_computation.1 | async-start | bytes 524288 | tf_op jit(solution)/shard_map/all_to_all | solution.py:343
  75.2 0.1 copy.24
  75.3 2.0 %collective-permute-start.18 = (bf16[16,256]{1,0:T(8,128)(2,1)S(1)}, bf16[16,256]{1,0:T(8,128)(2,1)S(1)}, u32[]{:S(2)}, u32[]{:S(2)}) collective-permute-start(bf16[16,256]{1,0:T(8,128)(2,1)S(1)} %get-tuple-element.48), channel_id=1, source_target_pairs={{0,2},{2,0},{4,6},{6,4},{8,10},{10,8},{12,14},{14,12},{16,18},{18,... | collective-permute-start | bytes 24584 | tf_op jit(solution)/shard_map/ppermute | solution.py:261
  77.3 1.5 %collective-permute-start.19 = (bf16[16,256]{1,0:T(8,128)(2,1)S(1)}, bf16[16,256]{1,0:T(8,128)(2,1)S(1)}, u32[]{:S(2)}, u32[]{:S(2)}) collective-permute-start(bf16[16,256]{1,0:T(8,128)(2,1)S(1)} %get-tuple-element.49), channel_id=1, source_target_pairs={{0,4},{2,6},{4,0},{6,2},{8,12},{10,14},{12,8},{14,10},{16,20},{18,... | collective-permute-start | bytes 24584 | tf_op jit(solution)/shard_map/ppermute | solution.py:261
  78.8 0.1 collective-permute-start.20
  78.9 0.1 compare_select_fusion
  79.0 0.1 copy.25.weight_ref
  79.0 0.7 collective-permute-done.18.refs_1_
  79.7 1.3 %collective-permute-done.19.refs_2_ = bf16[16,256]{1,0:T(8,128)(2,1)S(1)} collective-permute-done((bf16[16,256]{1,0:T(8,128)(2,1)S(1)}, bf16[16,256]{1,0:T(8,128)(2,1)S(1)}, u32[]{:S(2)}, u32[]{:S(2)}) %collective-permute-start.19) | collective-permute-done | bytes 8224 | tf_op jit(solution)/shard_map/ppermute | solution.py:261
  81.0 2.4 %collective-permute-done.20.refs_3_ = bf16[16,256]{1,0:T(8,128)(2,1)S(1)} collective-permute-done((bf16[16,256]{1,0:T(8,128)(2,1)S(1)}, bf16[16,256]{1,0:T(8,128)(2,1)S(1)}, u32[]{:S(2)}, u32[]{:S(2)}) %collective-permute-start.20) | collective-permute-done | bytes 8224 | tf_op jit(solution)/shard_map/ppermute | solution.py:261
  83.3 2.3 %all-to-all-done.1 = bf16[16,8,1024]{2,1,0:T(8,128)(2,1)S(1)} async-done(((bf16[16,8,1024]{2,1,0:T(8,128)(2,1)}), bf16[16,8,1024]{2,1,0:T(8,128)(2,1)S(1)}, u32[]{:S(2)}, u32[]{:S(2)}) %all-to-all-start.1) | async-done | bytes 262176 | tf_op jit(solution)/shard_map/all_to_all | solution.py:343
  85.6 0.8 shard_map.164
  (26 shorter events, 0.1 us)
Async XLA Ops:
  0.6 10.4 %copy-start.10 = (s32[16,2]{0,1:T(2,128)S(1)}, s32[16,2]{0,1:T(2,128)}, u32[]{:S(2)}) copy-start(s32[16,2]{0,1:T(2,128)} %param.25) | copy-start | bytes 388
  0.6 20.1 %copy-start.5 = (bf16[512,128]{1,0:T(8,128)(2,1)S(1)}, bf16[512,128]{1,0:T(8,128)(2,1)}, u32[]{:S(2)}) copy-start(bf16[512,128]{1,0:T(8,128)(2,1)} %refs_4_.3) | copy-start | bytes 393220
  0.7 24.9 %copy-start.7 = (f32[2048]{0:T(1024)S(1)}, f32[2048]{0:T(1024)}, u32[]{:S(2)}) copy-start(f32[2048]{0:T(1024)} %param.16) | copy-start | bytes 24580
  1.9 23.6 %collective-permute-start.5 = (bf16[128,1536]{1,0:T(8,128)(2,1)S(1)}, bf16[128,1536]{1,0:T(8,128)(2,1)S(1)}, u32[]{:S(2)}, u32[]{:S(2)}) collective-permute-start(bf16[128,1536]{1,0:T(8,128)(2,1)S(1)} %get-tuple-element.31.refs_5_), channel_id=1, source_target_pairs={{0,8},{2,10},{4,12},{6,14},{8,0},{10,2},{12,4},{14,6},{16,24},{18,... | collective-permute-start | bytes 1179656 | tf_op jit(solution)/shard_map/ppermute | solution.py:261
  5.1 20.5 %collective-permute-start.4 = (bf16[128,1536]{1,0:T(8,128)(2,1)S(1)}, bf16[128,1536]{1,0:T(8,128)(2,1)S(1)}, u32[]{:S(2)}, u32[]{:S(2)}) collective-permute-start(bf16[128,1536]{1,0:T(8,128)(2,1)S(1)} %get-tuple-element.31.refs_5_), channel_id=1, source_target_pairs={{0,4},{2,6},{4,0},{6,2},{8,12},{10,14},{12,8},{14,10},{16,20},{18,... | collective-permute-start | bytes 1179656 | tf_op jit(solution)/shard_map/ppermute | solution.py:261
  6.6 18.9 %collective-permute-start.3 = (bf16[128,1536]{1,0:T(8,128)(2,1)S(1)}, bf16[128,1536]{1,0:T(8,128)(2,1)S(1)}, u32[]{:S(2)}, u32[]{:S(2)}) collective-permute-start(bf16[128,1536]{1,0:T(8,128)(2,1)S(1)} %get-tuple-element.31.refs_5_), channel_id=1, source_target_pairs={{0,2},{2,0},{4,6},{6,4},{8,10},{10,8},{12,14},{14,12},{16,18},{18,... | collective-permute-start | bytes 1179656 | tf_op jit(solution)/shard_map/ppermute | solution.py:261
  8.1 9.0 %collective-permute-start = (bf16[16,512]{1,0:T(8,128)(2,1)S(1)}, bf16[16,512]{1,0:T(8,128)(2,1)S(1)}, u32[]{:S(2)}, u32[]{:S(2)}) collective-permute-start(bf16[16,512]{1,0:T(8,128)(2,1)S(1)} %get-tuple-element.28), channel_id=1, source_target_pairs={{0,14},{2,12},{4,10},{6,8},{8,6},{10,4},{12,2},{14,0},{16,30},{18,... | collective-permute-start | bytes 49160 | tf_op jit(solution)/shard_map/ppermute | solution.py:261
  8.1 12.7 %collective-permute-start.1 = (bf16[16,512]{1,0:T(8,128)(2,1)S(1)}, bf16[16,512]{1,0:T(8,128)(2,1)S(1)}, u32[]{:S(2)}, u32[]{:S(2)}) collective-permute-start(bf16[16,512]{1,0:T(8,128)(2,1)S(1)} %get-tuple-element.29), channel_id=1, source_target_pairs={{0,16},{2,18},{4,20},{6,22},{8,24},{10,26},{12,28},{14,30},{16,0},... | collective-permute-start | bytes 49160 | tf_op jit(solution)/shard_map/ppermute | solution.py:261
  17.0 7.6 %collective-permute-start.2 = (bf16[16,512]{1,0:T(8,128)(2,1)S(1)}, bf16[16,512]{1,0:T(8,128)(2,1)S(1)}, u32[]{:S(2)}, u32[]{:S(2)}) collective-permute-start(bf16[16,512]{1,0:T(8,128)(2,1)S(1)} %get-tuple-element.30), channel_id=1, source_target_pairs={{0,30},{2,28},{4,26},{6,24},{8,22},{10,20},{12,18},{14,16},{16,14}... | collective-permute-start | bytes 49160 | tf_op jit(solution)/shard_map/ppermute | solution.py:261
  20.7 24.6 %collective-permute-start.13 = (bf16[512,128]{1,0:T(8,128)(2,1)S(1)}, bf16[512,128]{1,0:T(8,128)(2,1)S(1)}, u32[]{:S(2)}, u32[]{:S(2)}) collective-permute-start(bf16[512,128]{1,0:T(8,128)(2,1)S(1)} %copy-done.5), channel_id=1, source_target_pairs={{0,16},{2,18},{4,20},{6,22},{8,24},{10,26},{12,28},{14,30},{16,0},... | collective-permute-start | bytes 393224 | tf_op jit(solution)/shard_map/ppermute | solution.py:261
  24.6 21.4 %collective-permute-start.12 = (bf16[512,128]{1,0:T(8,128)(2,1)S(1)}, bf16[512,128]{1,0:T(8,128)(2,1)S(1)}, u32[]{:S(2)}, u32[]{:S(2)}) collective-permute-start(bf16[512,128]{1,0:T(8,128)(2,1)S(1)} %copy-done.5), channel_id=1, source_target_pairs={{0,8},{2,10},{4,12},{6,14},{8,0},{10,2},{12,4},{14,6},{16,24},{18,... | collective-permute-start | bytes 393224 | tf_op jit(solution)/shard_map/ppermute | solution.py:261
  25.5 11.5 %copy-start.4 = (f32[16,4,128,128]{3,2,1,0:T(8,128)S(1)}, f32[16,4,128,128]{3,2,1,0:T(8,128)}, u32[]{:S(2)}) copy-start(f32[16,4,128,128]{3,2,1,0:T(8,128)} %refs_8_.1) | copy-start | bytes 12582916
  25.5 11.4 %copy-start.6 = (bf16[16,2048]{1,0:T(8,128)(2,1)S(1)}, bf16[16,2048]{1,0:T(8,128)(2,1)}, u32[]{:S(2)}) copy-start(bf16[16,2048]{1,0:T(8,128)(2,1)} %refs_4_.2) | copy-start | bytes 196612
  25.5 11.4 %copy-start.8 = (f32[512]{0:T(512)S(1)}, f32[512]{0:T(512)}, u32[]{:S(2)}) copy-start(f32[512]{0:T(512)} %param.20) | copy-start | bytes 6148
  25.6 11.4 %copy-start.9 = (f32[512]{0:T(512)S(1)}, f32[512]{0:T(512)}, u32[]{:S(2)}) copy-start(f32[512]{0:T(512)} %param.21) | copy-start | bytes 6148
  25.9 6.4 %collective-permute-start.6 = (bf16[16,1536]{1,0:T(8,128)(2,1)S(1)}, bf16[16,1536]{1,0:T(8,128)(2,1)S(1)}, u32[]{:S(2)}, u32[]{:S(2)}) collective-permute-start(bf16[16,1536]{1,0:T(8,128)(2,1)S(1)} %get-tuple-element.33), channel_id=1, source_target_pairs={{0,14},{2,12},{4,10},{6,8},{8,6},{10,4},{12,2},{14,0},{16,30},{18,... | collective-permute-start | bytes 147464 | tf_op jit(solution)/shard_map/ppermute | solution.py:261
  26.9 7.9 %collective-permute-start.7 = (bf16[16,1536]{1,0:T(8,128)(2,1)S(1)}, bf16[16,1536]{1,0:T(8,128)(2,1)S(1)}, u32[]{:S(2)}, u32[]{:S(2)}) collective-permute-start(bf16[16,1536]{1,0:T(8,128)(2,1)S(1)} %get-tuple-element.34), channel_id=1, source_target_pairs={{0,16},{2,18},{4,20},{6,22},{8,24},{10,26},{12,28},{14,30},{16,0},... | collective-permute-start | bytes 147464 | tf_op jit(solution)/shard_map/ppermute | solution.py:261
  29.2 7.8 %collective-permute-start.8 = (bf16[16,1536]{1,0:T(8,128)(2,1)S(1)}, bf16[16,1536]{1,0:T(8,128)(2,1)S(1)}, u32[]{:S(2)}, u32[]{:S(2)}) collective-permute-start(bf16[16,1536]{1,0:T(8,128)(2,1)S(1)} %get-tuple-element.35), channel_id=1, source_target_pairs={{0,30},{2,28},{4,26},{6,24},{8,22},{10,20},{12,18},{14,16},{16,14}... | collective-permute-start | bytes 147464 | tf_op jit(solution)/shard_map/ppermute | solution.py:261
  32.4 13.7 %collective-permute-start.14 = (bf16[512,128]{1,0:T(8,128)(2,1)S(1)}, bf16[512,128]{1,0:T(8,128)(2,1)S(1)}, u32[]{:S(2)}, u32[]{:S(2)}) collective-permute-start(bf16[512,128]{1,0:T(8,128)(2,1)S(1)} %copy-done.5), channel_id=1, source_target_pairs={{0,24},{2,26},{4,28},{6,30},{8,16},{10,18},{12,20},{14,22},{16,8},... | collective-permute-start | bytes 393224 | tf_op jit(solution)/shard_map/ppermute | solution.py:261
  42.5 3.9 %collective-permute-start.9 = (bf16[16,896]{1,0:T(8,128)(2,1)S(1)}, bf16[16,896]{1,0:T(8,128)(2,1)S(1)}, u32[]{:S(2)}, u32[]{:S(2)}) collective-permute-start(bf16[16,896]{1,0:T(8,128)(2,1)S(1)} %get-tuple-element.37), channel_id=1, source_target_pairs={{0,2},{2,0},{4,6},{6,4},{8,10},{10,8},{12,14},{14,12},{16,18},{18,... | collective-permute-start | bytes 86024 | tf_op jit(solution)/shard_map/ppermute | solution.py:261
  43.9 3.9 %collective-permute-start.10 = (bf16[16,896]{1,0:T(8,128)(2,1)S(1)}, bf16[16,896]{1,0:T(8,128)(2,1)S(1)}, u32[]{:S(2)}, u32[]{:S(2)}) collective-permute-start(bf16[16,896]{1,0:T(8,128)(2,1)S(1)} %get-tuple-element.38), channel_id=1, source_target_pairs={{0,4},{2,6},{4,0},{6,2},{8,12},{10,14},{12,8},{14,10},{16,20},{18,... | collective-permute-start | bytes 86024 | tf_op jit(solution)/shard_map/ppermute | solution.py:261
  45.3 4.8 %collective-permute-start.11 = (bf16[16,896]{1,0:T(8,128)(2,1)S(1)}, bf16[16,896]{1,0:T(8,128)(2,1)S(1)}, u32[]{:S(2)}, u32[]{:S(2)}) collective-permute-start(bf16[16,896]{1,0:T(8,128)(2,1)S(1)} %get-tuple-element.39), channel_id=1, source_target_pairs={{0,6},{2,4},{4,2},{6,0},{8,14},{10,12},{12,10},{14,8},{16,22},{18,... | collective-permute-start | bytes 86024 | tf_op jit(solution)/shard_map/ppermute | solution.py:261
  50.0 17.0 %copy-start.2 = (bf16[1,1024,2048]{2,1,0:T(8,128)(2,1)S(1)}, bf16[1,1024,2048]{2,1,0:T(8,128)(2,1)}, u32[]{:S(2)}) copy-start(bf16[1,1024,2048]{2,1,0:T(8,128)(2,1)} %down_ref.1) | copy-start | bytes 12582916
  50.3 1.3 %collective-permute-start.15 = (bf16[64,256]{1,0:T(8,128)(2,1)S(1)}, bf16[64,256]{1,0:T(8,128)(2,1)S(1)}, u32[]{:S(2)}, u32[]{:S(2)}) collective-permute-start(bf16[64,256]{1,0:T(8,128)(2,1)S(1)} %get-tuple-element.41), channel_id=1, source_target_pairs={{0,1},{1,0},{2,3},{3,2},{4,5},{5,4},{6,7},{7,6},{8,9},{9,8},{10,11... | collective-permute-start | bytes 98312 | tf_op jit(solution)/shard_map/ppermute | solution.py:264
  51.6 15.5 %copy-start = (bf16[1,2048,1024]{2,1,0:T(8,128)(2,1)S(1)}, bf16[1,2048,1024]{2,1,0:T(8,128)(2,1)}, u32[]{:S(2)}) copy-start(bf16[1,2048,1024]{2,1,0:T(8,128)(2,1)} %gate_ref.1) | copy-start | bytes 12582916
  51.6 15.5 %copy-start.1 = (bf16[1,2048,1024]{2,1,0:T(8,128)(2,1)S(1)}, bf16[1,2048,1024]{2,1,0:T(8,128)(2,1)}, u32[]{:S(2)}) copy-start(bf16[1,2048,1024]{2,1,0:T(8,128)(2,1)} %up_ref.1) | copy-start | bytes 12582916
  51.6 15.5 %copy-start.3 = (f32[2048]{0:T(1024)S(1)}, f32[2048]{0:T(1024)}, u32[]{:S(2)}) copy-start(f32[2048]{0:T(1024)} %param.24) | copy-start | bytes 24580
  65.5 1.5 %collective-permute-start.16 = (bf16[16,32,256]{2,1,0:T(8,128)(2,1)S(1)}, bf16[16,32,256]{2,1,0:T(8,128)(2,1)S(1)}, u32[]{:S(2)}, u32[]{:S(2)}) collective-permute-start(bf16[16,32,256]{2,1,0:T(8,128)(2,1)S(1)} %all_to_all.10.mine_ref), channel_id=1, source_target_pairs={{0,1},{1,0},{2,3},{3,2},{4,5},{5,4},{6,7},{7,6},{8,9},{9,8},{10,11... | collective-permute-start | bytes 786440 | tf_op jit(solution)/shard_map/ppermute | solution.py:264
  67.1 8.2 %copy-start.11 = (f32[16,2]{0,1:T(2,128)S(1)}, f32[16,2]{0,1:T(2,128)}, u32[]{:S(2)}) copy-start(f32[16,2]{0,1:T(2,128)} %param.26) | copy-start | bytes 388
  69.3 1.6 %collective-permute-start.17 = (bf16[128,1024]{1,0:T(8,128)(2,1)S(1)}, bf16[128,1024]{1,0:T(8,128)(2,1)S(1)}, u32[]{:S(2)}, u32[]{:S(2)}) collective-permute-start(bf16[128,1024]{1,0:T(8,128)(2,1)S(1)} %get-tuple-element.46), channel_id=1, source_target_pairs={{0,1},{1,0},{2,3},{3,2},{4,5},{5,4},{6,7},{7,6},{8,9},{9,8},{10,11... | collective-permute-start | bytes 786440 | tf_op jit(solution)/shard_map/ppermute | solution.py:264
  71.7 13.9 %all-to-all-start.1 = ((bf16[16,8,1024]{2,1,0:T(8,128)(2,1)}), bf16[16,8,1024]{2,1,0:T(8,128)(2,1)S(1)}, u32[]{:S(2)}, u32[]{:S(2)}) async-start(bf16[16,8,1024]{2,1,0:T(8,128)(2,1)} %fusion), calls=%async_computation.1 | async-start | bytes 524288 | tf_op jit(solution)/shard_map/all_to_all | solution.py:343
  75.3 4.4 %collective-permute-start.18 = (bf16[16,256]{1,0:T(8,128)(2,1)S(1)}, bf16[16,256]{1,0:T(8,128)(2,1)S(1)}, u32[]{:S(2)}, u32[]{:S(2)}) collective-permute-start(bf16[16,256]{1,0:T(8,128)(2,1)S(1)} %get-tuple-element.48), channel_id=1, source_target_pairs={{0,2},{2,0},{4,6},{6,4},{8,10},{10,8},{12,14},{14,12},{16,18},{18,... | collective-permute-start | bytes 24584 | tf_op jit(solution)/shard_map/ppermute | solution.py:261
  77.3 3.7 %collective-permute-start.19 = (bf16[16,256]{1,0:T(8,128)(2,1)S(1)}, bf16[16,256]{1,0:T(8,128)(2,1)S(1)}, u32[]{:S(2)}, u32[]{:S(2)}) collective-permute-start(bf16[16,256]{1,0:T(8,128)(2,1)S(1)} %get-tuple-element.49), channel_id=1, source_target_pairs={{0,4},{2,6},{4,0},{6,2},{8,12},{10,14},{12,8},{14,10},{16,20},{18,... | collective-permute-start | bytes 24584 | tf_op jit(solution)/shard_map/ppermute | solution.py:261
  78.8 4.5 %collective-permute-start.20 = (bf16[16,256]{1,0:T(8,128)(2,1)S(1)}, bf16[16,256]{1,0:T(8,128)(2,1)S(1)}, u32[]{:S(2)}, u32[]{:S(2)}) collective-permute-start(bf16[16,256]{1,0:T(8,128)(2,1)S(1)} %get-tuple-element.50), channel_id=1, source_target_pairs={{0,6},{2,4},{4,2},{6,0},{8,14},{10,12},{12,10},{14,8},{16,22},{18,... | collective-permute-start | bytes 24584 | tf_op jit(solution)/shard_map/ppermute | solution.py:261

commit v2 on v1

--- a/solution.py
+++ b/solution.py
@@ -11,7 +11,6 @@
 EXPERTS = 8
 TOP = 2
 LANES = 128
-SLOTS = 8
 
 
 epsilon = 1e-06
@@ -39,6 +38,30 @@
         compiler_params=pltpu.CompilerParams(vmem_limit_bytes=mib << 20),
         cost_estimate=pl.CostEstimate(flops=flops, bytes_accessed=traffic, transcendentals=0),
     )(*args)
+
+
+def thirds(values):
+    high = values.astype(jnp.bfloat16)
+    rest = values - high.astype(jnp.float32)
+    middle = rest.astype(jnp.bfloat16)
+    low = (rest - middle.astype(jnp.float32)).astype(jnp.bfloat16)
+    return high, middle, low
+
+
+def spreader(count):
+    shape = (3 * count, count * LANES)
+    row = lax.broadcasted_iota(jnp.int32, shape, 0) % count
+    col = lax.broadcasted_iota(jnp.int32, shape, 1) // LANES
+    return jnp.where(row == col, 1.0, 0.0).astype(jnp.bfloat16)
+
+
+def spread(values, matrix):
+    return lax.dot_general(
+        jnp.concatenate([part.astype(jnp.float32) for part in thirds(values)], axis=0).astype(jnp.bfloat16),
+        matrix,
+        (((0,), (0,)), ((), ())),
+        preferred_element_type=jnp.float32,
+    )
 
 
 def prep_kernel(coset, tokens_ref, *refs):
@@ -65,6 +88,32 @@
         copy.wait()
 
 
+def route_kernel(cap, span, ids_ref, weights_ref, info_ref, combine_ref):
+    count = ids_ref.shape[0]
+    ids, weights = ids_ref[...], weights_ref[...]
+    lane = lax.broadcasted_iota(jnp.int32, (count, LANES), 1)
+    picks = [ids[:, k : k + 1] == lane for k in range(TOP)]
+    chosen = functools.reduce(jnp.logical_or, picks)
+    earlier = lax.broadcasted_iota(jnp.int32, (count, count), 0) > lax.broadcasted_iota(
+        jnp.int32, (count, count), 1
+    )
+    rank = jnp.dot(
+        jnp.where(earlier, 1.0, 0.0).astype(jnp.bfloat16),
+        jnp.where(chosen, 1.0, 0.0).astype(jnp.bfloat16),
+        preferred_element_type=jnp.float32,
+    )
+    info_ref[...] = jnp.where(chosen, rank, 2.0 * count).astype(jnp.bfloat16)
+    column = lax.broadcasted_iota(jnp.int32, combine_ref.shape, 1)
+    expert = column // (span * GROUP * cap)
+    place = (column % cap).astype(jnp.float32)
+    total = jnp.zeros(combine_ref.shape, jnp.float32)
+    for k in range(TOP):
+        own = jnp.sum(jnp.where(picks[k], rank, 0.0), axis=-1, keepdims=True)
+        hit = (ids[:, k : k + 1] == expert) & (own == place)
+        total = total + jnp.where(hit, weights[:, k : k + 1], 0.0)
+    combine_ref[...] = total
+
+
 def project_kernel(group, *refs):
     token_refs, gain_ref, weight_refs, outs = (
         refs[:group],
@@ -86,17 +135,18 @@
         out[...] = total[m * count : (m + 1) * count].astype(out.dtype)
 
 
-def state_kernel(group, outer, *refs):
+def readout_kernel(group, outer, *refs):
     part_refs = refs[:group]
     tokens_ref, bound_ref, gain_ref, info_ref, state_ref = refs[group : group + 5]
-    new_ref = refs[group + 5]
-    payloads = refs[group + 6 :]
+    forget_ref, fresh_ref = refs[group + 5 : group + 7]
+    payloads = refs[group + 7 :]
     count = tokens_ref.shape[0]
     proj = bound_ref.shape[1]
     half = outer // 2
 
     tokens = tokens_ref[...].astype(jnp.float32)
     scale = lax.rsqrt(jnp.mean(tokens * tokens, axis=-1, keepdims=True) + epsilon)
+    matrix = spreader(count)
     for head in range(proj // LANES):
 
         def pick(which):
@@ -111,15 +161,15 @@
         forget = bound + (1.0 - bound) * jax.nn.sigmoid(pick(0))
         fresh = pick(1)
         query = pick(2)
-        forget_t = forget.T
-        query_t = query.T
-        rows = []
-        for s in range(count):
-            row = fresh[s : s + 1, :]
-            new = row + forget_t[:, s : s + 1] * (state_ref[s, head] - row)
-            new_ref[s, head] = new
-            rows.append(jnp.sum(query_t[:, s : s + 1] * new, axis=0, keepdims=True))
-        readout = jnp.concatenate(rows, axis=0)
+        forget_ref[:, cols] = forget
+        fresh_ref[:, cols] = fresh
+        kept = spread(query * forget, matrix)
+        rows = [
+            jnp.sum(kept[:, s * LANES : (s + 1) * LANES] * state_ref[s, head], axis=0, keepdims=True)
+            for s in range(count)
+        ]
+        added = jnp.sum(query * (1.0 - forget), axis=-1, keepdims=True) * fresh
+        readout = jnp.concatenate(rows, axis=0) + added
         normed = (
             readout
             * lax.rsqrt(jnp.mean(readout * readout, axis=-1, keepdims=True) + epsilon)
@@ -135,6 +185,14 @@
             block = (core * half + a) * GROUP + (place ^ m)
             out[:, proj + a * LANES : proj + (a + 1) * LANES] = tokens_ref[:, aligned(block * LANES, LANES)]
         out[:, proj + half * LANES :] = info_ref[...]
+
+
+def update_kernel(forget_ref, fresh_ref, state_ref, new_ref):
+    count = forget_ref.shape[0]
+    kept = spread(forget_ref[...], spreader(count))
+    for s in range(count):
+        keep = kept[:, s * LANES : (s + 1) * LANES]
+        new_ref[s, 0] = keep * state_ref[s, 0] + (1.0 - keep) * fresh_ref[s : s + 1, :]
 
 
 def mix_kernel(outer, *refs):
@@ -172,11 +230,12 @@
         ref[...] = after_ref[aligned((place ^ m) * count, count), :]
     after = after_ref[...]
     slots = info_ref[...].astype(jnp.float32).T
-    rows = GROUP * SLOTS
+    rows = out_ref.shape[1]
+    cap = rows // GROUP
     row = lax.broadcasted_iota(jnp.int32, (rows, after.shape[0]), 0)
     col = lax.broadcasted_iota(jnp.int32, (rows, after.shape[0]), 1)
-    same = (row // SLOTS) == (col // count)
-    slot = (row % SLOTS).astype(jnp.float32)
+    same = (row // cap) == (col // count)
+    slot = (row % cap).astype(jnp.float32)
     for e in range(EXPERTS):
         chosen = same & (slots[e : e + 1, :] == slot)
         select = jnp.where(chosen, 1.0, 0.0).astype(jnp.bfloat16)
@@ -188,8 +247,9 @@
 def expert_kernel(outer, mine_ref, theirs_ref, gain_ref, gate_ref, up_ref, down_ref, own_ref, other_ref, rows_ref, total_ref):
     core = lax.axis_index("tp")
     half = outer // 2
-    width = rows_ref.shape[1] // 2
-    block = GROUP * SLOTS
+    total_rows, width = rows_ref.shape[0], rows_ref.shape[1] // 2
+    block = mine_ref.shape[1]
+    cap = block // GROUP
     for ref, side in ((mine_ref, core), (theirs_ref, 1 - core)):
         for z in range(outer):
             for q in range(GROUP):
@@ -197,19 +257,33 @@
                     at = side * width + (a * GROUP + q) * LANES
                     rows_ref[z * block : (z + 1) * block, aligned(at, LANES)] = ref[
                         z * GROUP + q, :, a * LANES : (a + 1) * LANES
-                    ]
-    values = rows_ref[...].astype(jnp.float32)
+                    ].astype(jnp.float32)
+    values = rows_ref[...]
     scale = lax.rsqrt(jnp.mean(values * values, axis=-1, keepdims=True) + epsilon)
     rows = (values * scale * gain_ref[...]).astype(jnp.bfloat16)
     gate = jnp.dot(rows, gate_ref[0], preferred_element_type=jnp.float32)
     up = jnp.dot(rows, up_ref[0], preferred_element_type=jnp.float32)
     hidden = (jax.nn.silu(gate) * up).astype(jnp.bfloat16)
     total_ref[...] = jnp.dot(hidden, down_ref[0], preferred_element_type=jnp.float32).astype(jnp.bfloat16)
-    own_ref[...] = total_ref[:, aligned(core * width, width)]
-    other_ref[...] = total_ref[:, aligned((1 - core) * width, width)]
-
-
-def combine_kernel(outer, got_ref, weight_ref, *refs):
+    part = width // GROUP
+    tall = own_ref.shape[0]
+    row = lax.broadcasted_iota(jnp.int32, (tall, total_rows), 0)
+    col = lax.broadcasted_iota(jnp.int32, (tall, total_rows), 1)
+    source = (row // block) * cap + row % cap
+    piece = (row % block) // cap
+    selects = [
+        jnp.where((source == col) & (piece == k), 1.0, 0.0).astype(jnp.bfloat16) for k in range(GROUP)
+    ]
+    for ref, side in ((other_ref, 1 - core), (own_ref, core)):
+        packed = None
+        for k, select in enumerate(selects):
+            values = total_ref[:, aligned(side * width + k * part, part)]
+            term = jnp.dot(select, values, preferred_element_type=jnp.float32)
+            packed = term if packed is None else packed + term
+        ref[...] = packed.astype(jnp.bfloat16)
+
+
+def combine_kernel(outer, cap, got_ref, weight_ref, *refs):
     afters, out_ref, base_ref = refs[:GROUP], refs[GROUP], refs[GROUP + 1]
     place = lax.axis_index("ep") % GROUP
     half = outer // 2
@@ -218,15 +292,19 @@
             at = (a * GROUP + (place ^ m)) * LANES
             base_ref[:, aligned(at, LANES)] = ref[:, a * LANES : (a + 1) * LANES].astype(jnp.float32)
     weight = weight_ref[...]
-    high = weight.astype(jnp.bfloat16)
-    rest = weight - high.astype(jnp.float32)
-    middle = rest.astype(jnp.bfloat16)
-    low = (rest - middle.astype(jnp.float32)).astype(jnp.bfloat16)
     values = got_ref[...]
-    mix = jnp.dot(high, values, preferred_element_type=jnp.float32)
-    mix = mix + jnp.dot(middle, values, preferred_element_type=jnp.float32)
-    mix = mix + jnp.dot(low, values, preferred_element_type=jnp.float32)
-    out_ref[...] = (base_ref[...] + mix).astype(jnp.bfloat16)
+    _, part = values.shape
+    block = GROUP * cap
+    count = weight.shape[0]
+    piece = (lax.broadcasted_iota(jnp.int32, weight.shape, 1) % block) // cap
+    parts = thirds(weight)
+    for k in range(GROUP):
+        split = [jnp.where(piece == k, w.astype(jnp.float32), 0.0) for w in parts]
+        stacked = jnp.concatenate(split, axis=0).astype(jnp.bfloat16)
+        mix = jnp.dot(stacked, values, preferred_element_type=jnp.float32)
+        mix = mix[:count] + mix[count : 2 * count] + mix[2 * count :]
+        at = slice(k * part, (k + 1) * part)
+        out_ref[:, at] = (base_ref[:, at] + mix).astype(jnp.bfloat16)
 
 
 def fast_shards(
@@ -249,6 +327,7 @@
     bf16, f32 = jnp.bfloat16, jnp.float32
     ep = lax.axis_size("ep")
     count, width = tokens.shape
+    heads, size = state.shape[1], state.shape[2]
     proj = query_weight.shape[1]
     outer = ep // GROUP
     half = outer // 2
@@ -277,17 +356,13 @@
     token_blocks = [move(value, mask) for value, mask in zip(sent, coset)]
     out_weights = [move(out_weight, GROUP * m) for m in range(outer)]
 
-    experts = jnp.arange(EXPERTS, dtype=jnp.int32)
-    named = route_ids[:, :, None] == experts
-    chosen = jnp.any(named, axis=1)
-    before = (jnp.arange(count)[:, None] > jnp.arange(count)[None, :]).astype(f32)
-    rank = jnp.sum(before[:, :, None] * chosen.astype(f32)[None, :, :], axis=1)
-    slot_of = jnp.where(chosen, rank, 2.0 * SLOTS)
-    share = jnp.sum(jnp.where(named, route_weights[:, :, None], 0.0), axis=1)
-    info = jnp.pad(slot_of, ((0, 0), (0, LANES - EXPERTS))).astype(bf16)
-    places = jnp.arange(SLOTS, dtype=jnp.int32).astype(f32)
-    combine = jnp.where(slot_of[:, :, None, None] == places, share[:, :, None, None], 0.0)
-    combine = jnp.broadcast_to(combine, (count, EXPERTS, span, SLOTS)).reshape(count, ep * SLOTS)
+    cap = 3 * count // 8
+    rows_out = GROUP * cap
+    info, combine = call(
+        functools.partial(route_kernel, cap, span),
+        (route_ids, route_weights),
+        [shaped(count, LANES), shaped(count, ep * rows_out, dtype=f32)],
+    )
 
     parts = call(
         functools.partial(project_kernel, len(coset)),
@@ -305,11 +380,10 @@
         info,
         state,
     )
-    new_state, *payloads = call(
-        functools.partial(state_kernel, len(coset), outer),
+    forget, fresh, *payloads = call(
+        functools.partial(readout_kernel, len(coset), outer),
         args,
-        [shaped(*state.shape, dtype=f32)] + [shaped(count, pay)] * GROUP,
-        mib=14,
+        [shaped(count, proj, dtype=f32)] * 2 + [shaped(count, pay)] * GROUP,
     )
     payloads = [move(value, m) for m, value in enumerate(payloads)]
 
@@ -324,28 +398,41 @@
     outgoing, *afters = call(
         functools.partial(dispatch_kernel, span),
         (own, got, resid, infos),
-        [shaped(ep, GROUP * SLOTS, half * LANES)] + [shaped(count, half * LANES)] * GROUP,
+        [shaped(ep, rows_out, half * LANES)] + [shaped(count, half * LANES)] * GROUP,
         scratch=[pltpu.VMEM((tall, half * LANES), bf16)],
     )
     slot_rows = lax.all_to_all(outgoing, "ep", split_axis=0, concat_axis=0, tiled=True)
     afters = [move(value, m) for m, value in enumerate(afters)]
     other_rows = swap(slot_rows)
 
-    total_rows = ep * SLOTS
+    total_rows = ep * cap
+    tall = ep * rows_out
+    part = width // 2 // GROUP
     mine, theirs = call(
         functools.partial(expert_kernel, outer),
         (slot_rows, other_rows, ffn_gain.reshape(1, width), expert_gate, expert_up, expert_down),
-        [shaped(total_rows, width // 2)] * 2,
-        scratch=[pltpu.VMEM((total_rows, width), bf16), pltpu.VMEM((total_rows, width), bf16)],
+        [shaped(tall, part)] * 2,
+        scratch=[pltpu.VMEM((total_rows, width), f32), pltpu.VMEM((total_rows, width), bf16)],
         mib=24,
     )
     reduced = (mine.astype(f32) + swap(theirs).astype(f32)).astype(bf16)
     returned = lax.all_to_all(
-        reduced.reshape(ep, SLOTS, width // 2), "ep", split_axis=0, concat_axis=0, tiled=True
-    )
+        reduced.reshape(ep, rows_out, part), "ep", split_axis=0, concat_axis=0, tiled=True
+    )
+    block = pl.BlockSpec((count, 1, size, size), lambda h: (0, h, 0, 0))
+    column = pl.BlockSpec((count, size), lambda h: (0, h))
+    new_state = pl.pallas_call(
+        update_kernel,
+        out_shape=shaped(*state.shape, dtype=f32),
+        grid=(heads,),
+        in_specs=[column, column, block],
+        out_specs=block,
+        compiler_params=pltpu.CompilerParams(vmem_limit_bytes=12 << 20),
+        cost_estimate=pl.CostEstimate(flops=3_000_000_000, bytes_accessed=8_000_000, transcendentals=0),
+    )(forget, fresh, pltpu.with_memory_space_constraint(state, pltpu.HBM))
     mixed_out = call(
-        functools.partial(combine_kernel, outer),
-        (returned.reshape(total_rows, width // 2), combine, *afters),
+        functools.partial(combine_kernel, outer, cap),
+        (returned.reshape(tall, part), combine, *afters),
         shaped(count, width // 2),
         scratch=[pltpu.VMEM((count, width // 2), f32)],
     )
@@ -468,7 +555,7 @@
         and ep % 8 == 0
         and ep % EXPERTS == 0
         and tokens.shape[0] % 16 == 0
-        and 3 * tokens.shape[0] // 8 <= SLOTS
+        and 3 * tokens.shape[0] // 8 % 2 == 0
         and tokens.shape[1] == ep * LANES
         and query_weight.shape[0] == LANES
         and state.shape[2:] == (LANES, LANES)

time: 86.8 us -> 80.2 us (0.924)
  waiting for transfers between devices: 26.7 us -> 20 us
  Pallas kernels: 10.7 us -> 12.5 us
  blocking collectives: 13.7 us -> 12.4 us
    pallas_call x0 -> x1, Pallas kernels: none -> 5.24 us  [fast_shards(): pl.pallas_call(update_kernel, out_shape=shaped(*state.shape, dtype=f32),...]
    ppermute x18, waiting for transfers between devices: 20.3 us -> 15.9 us  [move(): return lax.ppermute(value, 'ep', xor_pairs(ep, mask))]
    pallas_call x7 -> x8, Pallas kernels: 10.7 us -> 7.24 us  [call(): pl.pallas_call(kernel, out_shape=outs, in_specs=[pl.BlockSpec(memory_spac...]
    all_to_all x1, waiting for transfers between devices: 2.3 us -> 0.07 us  [fast_shards(): lax.all_to_all(reduced.reshape(ep, rows_out, part), 'ep', split_axis=0, c...]
    all_to_all x1, blocking collectives: 13.7 us -> 12.4 us  [fast_shards(): lax.all_to_all(outgoing, 'ep', split_axis=0, concat_axis=0, tiled=True)]
  transfers between devices with their start and end apart: 22 -> 22, of which waited for: 13 -> 10; matrix products, arithmetic and copies ran while one was open for 0% -> 0% of each run, Pallas kernels for 7% -> 9%
where the time goes in v2:
time: 80.2 us; the launch traced here: 79.8 us
  starting transfers between devices  33.3 us (42%)
  waiting for transfers between devices  20 us (25%)
  Pallas kernels  12.5 us (16%)
  blocking collectives  12.4 us (15%)
  between operations  0.81 us (1%)
    ppermute x18, starting transfers between devices, move(): return lax.ppermute(value, 'ep', xor_pairs(ep, mask))  29.5 us
    ppermute x18, waiting for transfers between devices, move(): return lax.ppermute(value, 'ep', xor_pairs(ep, mask))  15.9 us
    all_to_all x1, blocking collectives, fast_shards(): lax.all_to_all(outgoing, 'ep', split_axis=0, concat_axis=0, tiled=True)  12.4 us
    pallas_call x8, Pallas kernels, call(): pl.pallas_call(kernel, out_shape=outs, in_specs=[pl.BlockSpec(memory_spac...  7.24 us
    pallas_call x1, Pallas kernels, fast_shards(): pl.pallas_call(update_kernel, out_shape=shaped(*state.shape, dtype=f32),...  5.24 us
    ppermute x3, waiting for transfers between devices, swap(): return lax.ppermute(value, 'tp', [(0, 1), (1, 0)])  3.94 us
    all_to_all x1, starting transfers between devices, fast_shards(): lax.all_to_all(reduced.reshape(ep, rows_out, part), 'ep', split_axis=0, c...  3.52 us
  transfers between devices with their start and end apart: 22, of which 10 were waited for; matrix products, arithmetic and copies ran while one was open for 0% of the time, Pallas kernels for 9%

profile of v2, /device:TPU:0, one launch (start us, length us, event | category | flops | bytes accessed | tf_op | source)
XLA Modules:
  0.0 79.8 jit_solution(9613924008712730241)
XLA Ops:
  0.6 0.0 copy-start.10
  0.6 0.0 copy-start.11
  0.7 0.0 copy-start.5
  0.7 0.0 copy-start.7
  0.7 1.3 %shard_map.158 = (bf16[128,1536]{1,0:T(8,128)(2,1)S(1)}, bf16[16,512]{1,0:T(8,128)(2,1)S(1)}, bf16[16,512]{1,0:T(8,128)(2,1)S(1)}, bf16[16,512]{1,0:T(8,128)(2,1)S(1)}, bf16[16,512]{1,0:T(8,128)(2,1)S(1)}) custom-call(bf16[16,2048]{1,0:T(8,128)(2,1)} %refs_4_.2, bf16[128,512]{1,0:T(8,128)(2,1)} %refs_0_.1, bf16[128,512]{1,0:T(8,128)(2,1)} %refs_1_.1, ...), custom_call_target="tpu_custom_call" | custom-call | flops 3000000000 | bytes 100000 | tf_op jit(solution)/shard_map/pallas_call | solution.py:32
  1.9 3.1 %collective-permute-start.5 = (bf16[128,1536]{1,0:T(8,128)(2,1)S(1)}, bf16[128,1536]{1,0:T(8,128)(2,1)S(1)}, u32[]{:S(2)}, u32[]{:S(2)}) collective-permute-start(bf16[128,1536]{1,0:T(8,128)(2,1)S(1)} %get-tuple-element.34.refs_5_), channel_id=1, source_target_pairs={{0,8},{2,10},{4,12},{6,14},{8,0},{10,2},{12,4},{14,6},{16,24},{18,... | collective-permute-start | bytes 1179656 | tf_op jit(solution)/shard_map/ppermute | solution.py:340
  5.1 1.5 %collective-permute-start.4 = (bf16[128,1536]{1,0:T(8,128)(2,1)S(1)}, bf16[128,1536]{1,0:T(8,128)(2,1)S(1)}, u32[]{:S(2)}, u32[]{:S(2)}) collective-permute-start(bf16[128,1536]{1,0:T(8,128)(2,1)S(1)} %get-tuple-element.34.refs_5_), channel_id=1, source_target_pairs={{0,4},{2,6},{4,0},{6,2},{8,12},{10,14},{12,8},{14,10},{16,20},{18,... | collective-permute-start | bytes 1179656 | tf_op jit(solution)/shard_map/ppermute | solution.py:340
  6.6 1.5 %collective-permute-start.3 = (bf16[128,1536]{1,0:T(8,128)(2,1)S(1)}, bf16[128,1536]{1,0:T(8,128)(2,1)S(1)}, u32[]{:S(2)}, u32[]{:S(2)}) collective-permute-start(bf16[128,1536]{1,0:T(8,128)(2,1)S(1)} %get-tuple-element.34.refs_5_), channel_id=1, source_target_pairs={{0,2},{2,0},{4,6},{6,4},{8,10},{10,8},{12,14},{14,12},{16,18},{18,... | collective-permute-start | bytes 1179656 | tf_op jit(solution)/shard_map/ppermute | solution.py:340
  8.1 0.0 collective-permute-start
  8.1 2.9 %collective-permute-start.1 = (bf16[16,512]{1,0:T(8,128)(2,1)S(1)}, bf16[16,512]{1,0:T(8,128)(2,1)S(1)}, u32[]{:S(2)}, u32[]{:S(2)}) collective-permute-start(bf16[16,512]{1,0:T(8,128)(2,1)S(1)} %get-tuple-element.32), channel_id=1, source_target_pairs={{0,16},{2,18},{4,20},{6,22},{8,24},{10,26},{12,28},{14,30},{16,0},... | collective-permute-start | bytes 49160 | tf_op jit(solution)/shard_map/ppermute | solution.py:340
  11.0 6.0 %collective-permute-done.refs_1_ = bf16[16,512]{1,0:T(8,128)(2,1)S(1)} collective-permute-done((bf16[16,512]{1,0:T(8,128)(2,1)S(1)}, bf16[16,512]{1,0:T(8,128)(2,1)S(1)}, u32[]{:S(2)}, u32[]{:S(2)}) %collective-permute-start) | collective-permute-done | bytes 16416 | tf_op jit(solution)/shard_map/ppermute | solution.py:340
  17.0 3.5 %collective-permute-start.2 = (bf16[16,512]{1,0:T(8,128)(2,1)S(1)}, bf16[16,512]{1,0:T(8,128)(2,1)S(1)}, u32[]{:S(2)}, u32[]{:S(2)}) collective-permute-start(bf16[16,512]{1,0:T(8,128)(2,1)S(1)} %get-tuple-element.33), channel_id=1, source_target_pairs={{0,30},{2,28},{4,26},{6,24},{8,22},{10,20},{12,18},{14,16},{16,14}... | collective-permute-start | bytes 49160 | tf_op jit(solution)/shard_map/ppermute | solution.py:340
  20.5 0.0 copy-done.10
  20.6 0.1 copy.17.ids_ref
  20.6 0.1 copy.18.weights_ref
  20.7 0.0 collective-permute-done.1.refs_2_
  20.7 0.0 copy-done.5
  20.7 0.0 collective-permute-start.13
  20.8 3.9 %collective-permute-done.2.refs_3_ = bf16[16,512]{1,0:T(8,128)(2,1)S(1)} collective-permute-done((bf16[16,512]{1,0:T(8,128)(2,1)S(1)}, bf16[16,512]{1,0:T(8,128)(2,1)S(1)}, u32[]{:S(2)}, u32[]{:S(2)}) %collective-permute-start.2) | collective-permute-done | bytes 16416 | tf_op jit(solution)/shard_map/ppermute | solution.py:340
  24.6 0.8 %collective-permute-start.12 = (bf16[512,128]{1,0:T(8,128)(2,1)S(1)}, bf16[512,128]{1,0:T(8,128)(2,1)S(1)}, u32[]{:S(2)}, u32[]{:S(2)}) collective-permute-start(bf16[512,128]{1,0:T(8,128)(2,1)S(1)} %copy-done.5), channel_id=1, source_target_pairs={{0,8},{2,10},{4,12},{6,14},{8,0},{10,2},{12,4},{14,6},{16,24},{18,... | collective-permute-start | bytes 393224 | tf_op jit(solution)/shard_map/ppermute | solution.py:340
  25.5 0.0 collective-permute-done.5.refs_8_
  25.5 0.0 collective-permute-done.4.refs_7_
  25.5 0.0 collective-permute-done.3.refs_6_
  25.5 0.4 shard_map.159
  25.9 1.0 %collective-permute-start.6 = (bf16[16,1536]{1,0:T(8,128)(2,1)S(1)}, bf16[16,1536]{1,0:T(8,128)(2,1)S(1)}, u32[]{:S(2)}, u32[]{:S(2)}) collective-permute-start(bf16[16,1536]{1,0:T(8,128)(2,1)S(1)} %get-tuple-element.36), channel_id=1, source_target_pairs={{0,14},{2,12},{4,10},{6,8},{8,6},{10,4},{12,2},{14,0},{16,30},{18,... | collective-permute-start | bytes 147464 | tf_op jit(solution)/shard_map/ppermute | solution.py:340
  26.9 2.3 %collective-permute-start.7 = (bf16[16,1536]{1,0:T(8,128)(2,1)S(1)}, bf16[16,1536]{1,0:T(8,128)(2,1)S(1)}, u32[]{:S(2)}, u32[]{:S(2)}) collective-permute-start(bf16[16,1536]{1,0:T(8,128)(2,1)S(1)} %get-tuple-element.37), channel_id=1, source_target_pairs={{0,16},{2,18},{4,20},{6,22},{8,24},{10,26},{12,28},{14,30},{16,0},... | collective-permute-start | bytes 147464 | tf_op jit(solution)/shard_map/ppermute | solution.py:340
  29.2 3.3 %collective-permute-start.8 = (bf16[16,1536]{1,0:T(8,128)(2,1)S(1)}, bf16[16,1536]{1,0:T(8,128)(2,1)S(1)}, u32[]{:S(2)}, u32[]{:S(2)}) collective-permute-start(bf16[16,1536]{1,0:T(8,128)(2,1)S(1)} %get-tuple-element.38), channel_id=1, source_target_pairs={{0,30},{2,28},{4,26},{6,24},{8,22},{10,20},{12,18},{14,16},{16,14}... | collective-permute-start | bytes 147464 | tf_op jit(solution)/shard_map/ppermute | solution.py:340
  32.4 0.3 shard_map.160
  32.7 0.0 collective-permute-done.6.refs_1_
  32.7 2.4 %collective-permute-start.14 = (bf16[512,128]{1,0:T(8,128)(2,1)S(1)}, bf16[512,128]{1,0:T(8,128)(2,1)S(1)}, u32[]{:S(2)}, u32[]{:S(2)}) collective-permute-start(bf16[512,128]{1,0:T(8,128)(2,1)S(1)} %copy-done.5), channel_id=1, source_target_pairs={{0,24},{2,26},{4,28},{6,30},{8,16},{10,18},{12,20},{14,22},{16,8},... | collective-permute-start | bytes 393224 | tf_op jit(solution)/shard_map/ppermute | solution.py:340
  35.1 0.0 collective-permute-done.7.refs_2_
  35.1 1.8 %collective-permute-done.8.refs_3_ = bf16[16,1536]{1,0:T(8,128)(2,1)S(1)} collective-permute-done((bf16[16,1536]{1,0:T(8,128)(2,1)S(1)}, bf16[16,1536]{1,0:T(8,128)(2,1)S(1)}, u32[]{:S(2)}, u32[]{:S(2)}) %collective-permute-start.8) | collective-permute-done | bytes 49184 | tf_op jit(solution)/shard_map/ppermute | solution.py:340
  36.9 0.0 copy-done.4
  37.0 1.0 %shard_map.161 = (f32[16,512]{1,0:T(8,128)S(1)}, f32[16,512]{1,0:T(8,128)S(1)}, bf16[16,896]{1,0:T(8,128)(2,1)S(1)}, bf16[16,896]{1,0:T(8,128)(2,1)S(1)}, bf16[1...) custom-call(bf16[16,1536]{1,0:T(8,128)(2,1)S(1)} %get-tuple-element.35.refs_0_, ...), custom_call_target="tpu_custom_call" | custom-call | flops 3000000000 | bytes 100000 | tf_op jit(solution)/shard_map/pallas_call | solution.py:32
  37.9 1.4 %collective-permute-start.9 = (bf16[16,896]{1,0:T(8,128)(2,1)S(1)}, bf16[16,896]{1,0:T(8,128)(2,1)S(1)}, u32[]{:S(2)}, u32[]{:S(2)}) collective-permute-start(bf16[16,896]{1,0:T(8,128)(2,1)S(1)} %get-tuple-element.41), channel_id=1, source_target_pairs={{0,2},{2,0},{4,6},{6,4},{8,10},{10,8},{12,14},{14,12},{16,18},{18,... | collective-permute-start | bytes 86024 | tf_op jit(solution)/shard_map/ppermute | solution.py:340
  39.4 1.5 %collective-permute-start.10 = (bf16[16,896]{1,0:T(8,128)(2,1)S(1)}, bf16[16,896]{1,0:T(8,128)(2,1)S(1)}, u32[]{:S(2)}, u32[]{:S(2)}) collective-permute-start(bf16[16,896]{1,0:T(8,128)(2,1)S(1)} %get-tuple-element.42), channel_id=1, source_target_pairs={{0,4},{2,6},{4,0},{6,2},{8,12},{10,14},{12,8},{14,10},{16,20},{18,... | collective-permute-start | bytes 86024 | tf_op jit(solution)/shard_map/ppermute | solution.py:340
  40.9 0.0 collective-permute-done.13.refs_6_
  40.9 0.6 collective-permute-start.11
  41.4 0.0 collective-permute-done.12.refs_5_
  41.4 0.0 collective-permute-done.14.refs_7_
  41.4 0.4 collective-permute-done.9.refs_1_
  41.8 1.4 %collective-permute-done.10.refs_2_ = bf16[16,896]{1,0:T(8,128)(2,1)S(1)} collective-permute-done((bf16[16,896]{1,0:T(8,128)(2,1)S(1)}, bf16[16,896]{1,0:T(8,128)(2,1)S(1)}, u32[]{:S(2)}, u32[]{:S(2)}) %collective-permute-start.10) | collective-permute-done | bytes 28704 | tf_op jit(solution)/shard_map/ppermute | solution.py:340
  43.2 2.4 %collective-permute-done.11.refs_3_ = bf16[16,896]{1,0:T(8,128)(2,1)S(1)} collective-permute-done((bf16[16,896]{1,0:T(8,128)(2,1)S(1)}, bf16[16,896]{1,0:T(8,128)(2,1)S(1)}, u32[]{:S(2)}, u32[]{:S(2)}) %collective-permute-start.11) | collective-permute-done | bytes 28704 | tf_op jit(solution)/shard_map/ppermute | solution.py:340
  45.6 0.2 shard_map.162
  45.9 0.1 collective-permute-start.15
  46.0 1.2 %collective-permute-done.15.got_ref = bf16[64,256]{1,0:T(8,128)(2,1)S(1)} collective-permute-done((bf16[64,256]{1,0:T(8,128)(2,1)S(1)}, bf16[64,256]{1,0:T(8,128)(2,1)S(1)}, u32[]{:S(2)}, u32[]{:S(2)}) %collective-permute-start.15) | collective-permute-done | bytes 32800 | tf_op jit(solution)/shard_map/ppermute | solution.py:343
  47.2 0.2 shard_map.163
  47.4 12.4 %all_to_all.10.mine_ref = bf16[16,24,256]{2,1,0:T(8,128)(2,1)S(1)} all-to-all(bf16[16,24,256]{2,1,0:T(8,128)(2,1)S(1)} %get-tuple-element.48), channel_id=1, replica_groups=mesh['ep'=16,'tp'=2] {'ep'}, dimensions={0} | all-to-all | bytes 393216 | tf_op jit(solution)/shard_map/all_to_all | solution.py:404
  59.8 0.0 collective-permute-start.16
  59.8 1.4 %collective-permute-done.16.theirs_ref = bf16[16,24,256]{2,1,0:T(8,128)(2,1)S(1)} collective-permute-done((bf16[16,24,256]{2,1,0:T(8,128)(2,1)S(1)}, bf16[16,24,256]{2,1,0:T(8,128)(2,1)S(1)}, u32[]{:S(2)}, u32[]{:S(2)}) %collective-permute-start.16) | collective-permute-done | bytes 196640 | tf_op jit(solution)/shard_map/ppermute | solution.py:343
  61.3 3.1 %shard_map.164 = (bf16[384,256]{1,0:T(8,128)(2,1)S(1)}, bf16[384,256]{1,0:T(8,128)(2,1)S(1)}) custom-call(bf16[16,24,256]{2,1,0:T(8,128)(2,1)S(1)} %all_to_all.10.mine_ref, bf16[16,24,256]{2,1,0:T(8,128)(2,1)S(1)} %collective-permute-done.16.theirs_ref, f32[1,2048]{1,0:T(1,128)S(1)} %bitcast.7, bf16[1,2048,1024]{2,1,0:T(8,128)(2,1)S(1)} %copy-done, ...), custom_call_target="tpu_custom_call" | custom-call | flops 3000000000 | bytes 100000 | tf_op jit(solution)/shard_map/pallas_call | solution.py:32
  64.3 0.2 collective-permute-start.17
  64.5 1.3 %collective-permute-done.17 = bf16[384,256]{1,0:T(8,128)(2,1)S(1)} collective-permute-done((bf16[384,256]{1,0:T(8,128)(2,1)S(1)}, bf16[384,256]{1,0:T(8,128)(2,1)S(1)}, u32[]{:S(2)}, u32[]{:S(2)}) %collective-permute-start.17) | collective-permute-done | bytes 196640 | tf_op jit(solution)/shard_map/ppermute | solution.py:343
  65.8 0.7 add_convert_fusion
  66.6 3.5 %all-to-all-start.1 = ((bf16[16,24,256]{2,1,0:T(8,128)(2,1)}), bf16[16,24,256]{2,1,0:T(8,128)(2,1)S(1)}, u32[]{:S(2)}, u32[]{:S(2)}) async-start(bf16[16,24,256]{2,1,0:T(8,128)(2,1)} %bitcast.4), calls=%async_computation.1 | async-start | bytes 393216 | tf_op jit(solution)/shard_map/all_to_all | solution.py:419
  70.1 1.8 %collective-permute-start.18 = (bf16[16,256]{1,0:T(8,128)(2,1)S(1)}, bf16[16,256]{1,0:T(8,128)(2,1)S(1)}, u32[]{:S(2)}, u32[]{:S(2)}) collective-permute-start(bf16[16,256]{1,0:T(8,128)(2,1)S(1)} %get-tuple-element.53), channel_id=1, source_target_pairs={{0,2},{2,0},{4,6},{6,4},{8,10},{10,8},{12,14},{14,12},{16,18},{18,... | collective-permute-start | bytes 24584 | tf_op jit(solution)/shard_map/ppermute | solution.py:340
  71.9 1.5 %collective-permute-start.19 = (bf16[16,256]{1,0:T(8,128)(2,1)S(1)}, bf16[16,256]{1,0:T(8,128)(2,1)S(1)}, u32[]{:S(2)}, u32[]{:S(2)}) collective-permute-start(bf16[16,256]{1,0:T(8,128)(2,1)S(1)} %get-tuple-element.54), channel_id=1, source_target_pairs={{0,4},{2,6},{4,0},{6,2},{8,12},{10,14},{12,8},{14,10},{16,20},{18,... | collective-permute-start | bytes 24584 | tf_op jit(solution)/shard_map/ppermute | solution.py:340
  73.4 0.3 collective-permute-start.20
  73.7 5.2 %shard_map.166 = f32[16,4,128,128]{3,2,1,0:T(8,128)} custom-call(f32[16,512]{1,0:T(8,128)S(1)} %get-tuple-element.56.forget_ref, f32[16,512]{1,0:T(8,128)S(1)} %get-tuple-element.57.fresh_ref, f32[16,4,128,128]{3,2,1,0:T(8,128)} %state_ref.1), custom_call_target="tpu_custom_call" | custom-call | flops 3000000000 | bytes 8000000 | tf_op jit(solution)/shard_map/pallas_call | solution.py:424
  78.9 0.0 collective-permute-done.18.refs_1_
  78.9 0.0 collective-permute-done.19.refs_2_
  78.9 0.0 collective-permute-done.20.refs_3_
  78.9 0.1 all-to-all-done.1
  79.0 0.9 %shard_map.165 = bf16[16,1024]{1,0:T(8,128)(2,1)} custom-call(bf16[384,256]{1,0:T(8,128)(2,1)S(1)} %bitcast.6, f32[16,384]{1,0:T(8,128)S(1)} %get-tuple-element.51.weight_ref, bf16[16,256]{1,0:T(8,128)(2,1)S(1)} %get-tuple-element.52.refs_0_, bf16[16,256]{1,0:T(8,128)(2,1)S(1)} %collective-permute-done.18.refs_1_, ...), custom_call_target="tpu_custom_call" | custom-call | flops 3000000000 | bytes 100000 | tf_op jit(solution)/shard_map/pallas_call | solution.py:32
  (17 shorter events, 0.0 us)
Async XLA Ops:
  0.6 19.9 %copy-start.10 = (s32[16,2]{0,1:T(2,128)S(1)}, s32[16,2]{0,1:T(2,128)}, u32[]{:S(2)}) copy-start(s32[16,2]{0,1:T(2,128)} %param.25) | copy-start | bytes 388
  0.6 20.0 %copy-start.11 = (f32[16,2]{0,1:T(2,128)S(1)}, f32[16,2]{0,1:T(2,128)}, u32[]{:S(2)}) copy-start(f32[16,2]{0,1:T(2,128)} %param.26) | copy-start | bytes 388
  0.7 20.1 %copy-start.5 = (bf16[512,128]{1,0:T(8,128)(2,1)S(1)}, bf16[512,128]{1,0:T(8,128)(2,1)}, u32[]{:S(2)}) copy-start(bf16[512,128]{1,0:T(8,128)(2,1)} %refs_4_.3) | copy-start | bytes 393220
  0.7 24.8 %copy-start.7 = (f32[2048]{0:T(1024)S(1)}, f32[2048]{0:T(1024)}, u32[]{:S(2)}) copy-start(f32[2048]{0:T(1024)} %param.16) | copy-start | bytes 24580
  1.9 23.5 %collective-permute-start.5 = (bf16[128,1536]{1,0:T(8,128)(2,1)S(1)}, bf16[128,1536]{1,0:T(8,128)(2,1)S(1)}, u32[]{:S(2)}, u32[]{:S(2)}) collective-permute-start(bf16[128,1536]{1,0:T(8,128)(2,1)S(1)} %get-tuple-element.34.refs_5_), channel_id=1, source_target_pairs={{0,8},{2,10},{4,12},{6,14},{8,0},{10,2},{12,4},{14,6},{16,24},{18,... | collective-permute-start | bytes 1179656 | tf_op jit(solution)/shard_map/ppermute | solution.py:340
  5.1 20.4 %collective-permute-start.4 = (bf16[128,1536]{1,0:T(8,128)(2,1)S(1)}, bf16[128,1536]{1,0:T(8,128)(2,1)S(1)}, u32[]{:S(2)}, u32[]{:S(2)}) collective-permute-start(bf16[128,1536]{1,0:T(8,128)(2,1)S(1)} %get-tuple-element.34.refs_5_), channel_id=1, source_target_pairs={{0,4},{2,6},{4,0},{6,2},{8,12},{10,14},{12,8},{14,10},{16,20},{18,... | collective-permute-start | bytes 1179656 | tf_op jit(solution)/shard_map/ppermute | solution.py:340
  6.6 18.9 %collective-permute-start.3 = (bf16[128,1536]{1,0:T(8,128)(2,1)S(1)}, bf16[128,1536]{1,0:T(8,128)(2,1)S(1)}, u32[]{:S(2)}, u32[]{:S(2)}) collective-permute-start(bf16[128,1536]{1,0:T(8,128)(2,1)S(1)} %get-tuple-element.34.refs_5_), channel_id=1, source_target_pairs={{0,2},{2,0},{4,6},{6,4},{8,10},{10,8},{12,14},{14,12},{16,18},{18,... | collective-permute-start | bytes 1179656 | tf_op jit(solution)/shard_map/ppermute | solution.py:340
  8.1 9.0 %collective-permute-start = (bf16[16,512]{1,0:T(8,128)(2,1)S(1)}, bf16[16,512]{1,0:T(8,128)(2,1)S(1)}, u32[]{:S(2)}, u32[]{:S(2)}) collective-permute-start(bf16[16,512]{1,0:T(8,128)(2,1)S(1)} %get-tuple-element.31), channel_id=1, source_target_pairs={{0,14},{2,12},{4,10},{6,8},{8,6},{10,4},{12,2},{14,0},{16,30},{18,... | collective-permute-start | bytes 49160 | tf_op jit(solution)/shard_map/ppermute | solution.py:340
  8.1 12.6 %collective-permute-start.1 = (bf16[16,512]{1,0:T(8,128)(2,1)S(1)}, bf16[16,512]{1,0:T(8,128)(2,1)S(1)}, u32[]{:S(2)}, u32[]{:S(2)}) collective-permute-start(bf16[16,512]{1,0:T(8,128)(2,1)S(1)} %get-tuple-element.32), channel_id=1, source_target_pairs={{0,16},{2,18},{4,20},{6,22},{8,24},{10,26},{12,28},{14,30},{16,0},... | collective-permute-start | bytes 49160 | tf_op jit(solution)/shard_map/ppermute | solution.py:340
  17.0 7.6 %collective-permute-start.2 = (bf16[16,512]{1,0:T(8,128)(2,1)S(1)}, bf16[16,512]{1,0:T(8,128)(2,1)S(1)}, u32[]{:S(2)}, u32[]{:S(2)}) collective-permute-start(bf16[16,512]{1,0:T(8,128)(2,1)S(1)} %get-tuple-element.33), channel_id=1, source_target_pairs={{0,30},{2,28},{4,26},{6,24},{8,22},{10,20},{12,18},{14,16},{16,14}... | collective-permute-start | bytes 49160 | tf_op jit(solution)/shard_map/ppermute | solution.py:340
  20.7 20.1 %collective-permute-start.13 = (bf16[512,128]{1,0:T(8,128)(2,1)S(1)}, bf16[512,128]{1,0:T(8,128)(2,1)S(1)}, u32[]{:S(2)}, u32[]{:S(2)}) collective-permute-start(bf16[512,128]{1,0:T(8,128)(2,1)S(1)} %copy-done.5), channel_id=1, source_target_pairs={{0,16},{2,18},{4,20},{6,22},{8,24},{10,26},{12,28},{14,30},{16,0},... | collective-permute-start | bytes 393224 | tf_op jit(solution)/shard_map/ppermute | solution.py:340
  24.6 16.8 %collective-permute-start.12 = (bf16[512,128]{1,0:T(8,128)(2,1)S(1)}, bf16[512,128]{1,0:T(8,128)(2,1)S(1)}, u32[]{:S(2)}, u32[]{:S(2)}) collective-permute-start(bf16[512,128]{1,0:T(8,128)(2,1)S(1)} %copy-done.5), channel_id=1, source_target_pairs={{0,8},{2,10},{4,12},{6,14},{8,0},{10,2},{12,4},{14,6},{16,24},{18,... | collective-permute-start | bytes 393224 | tf_op jit(solution)/shard_map/ppermute | solution.py:340
  25.9 6.8 %collective-permute-start.6 = (bf16[16,1536]{1,0:T(8,128)(2,1)S(1)}, bf16[16,1536]{1,0:T(8,128)(2,1)S(1)}, u32[]{:S(2)}, u32[]{:S(2)}) collective-permute-start(bf16[16,1536]{1,0:T(8,128)(2,1)S(1)} %get-tuple-element.36), channel_id=1, source_target_pairs={{0,14},{2,12},{4,10},{6,8},{8,6},{10,4},{12,2},{14,0},{16,30},{18,... | collective-permute-start | bytes 147464 | tf_op jit(solution)/shard_map/ppermute | solution.py:340
  26.9 8.3 %collective-permute-start.7 = (bf16[16,1536]{1,0:T(8,128)(2,1)S(1)}, bf16[16,1536]{1,0:T(8,128)(2,1)S(1)}, u32[]{:S(2)}, u32[]{:S(2)}) collective-permute-start(bf16[16,1536]{1,0:T(8,128)(2,1)S(1)} %get-tuple-element.37), channel_id=1, source_target_pairs={{0,16},{2,18},{4,20},{6,22},{8,24},{10,26},{12,28},{14,30},{16,0},... | collective-permute-start | bytes 147464 | tf_op jit(solution)/shard_map/ppermute | solution.py:340
  29.1 7.8 %copy-start.4 = (f32[16,4,128,128]{3,2,1,0:T(8,128)S(1)}, f32[16,4,128,128]{3,2,1,0:T(8,128)}, u32[]{:S(2)}) copy-start(f32[16,4,128,128]{3,2,1,0:T(8,128)} %state_ref.1) | copy-start | bytes 12582916
  29.1 7.8 %copy-start.6 = (bf16[16,2048]{1,0:T(8,128)(2,1)S(1)}, bf16[16,2048]{1,0:T(8,128)(2,1)}, u32[]{:S(2)}) copy-start(bf16[16,2048]{1,0:T(8,128)(2,1)} %refs_4_.2) | copy-start | bytes 196612
  29.1 7.8 %copy-start.8 = (f32[512]{0:T(512)S(1)}, f32[512]{0:T(512)}, u32[]{:S(2)}) copy-start(f32[512]{0:T(512)} %param.20) | copy-start | bytes 6148
  29.1 7.8 %copy-start.9 = (f32[512]{0:T(512)S(1)}, f32[512]{0:T(512)}, u32[]{:S(2)}) copy-start(f32[512]{0:T(512)} %param.21) | copy-start | bytes 6148
  29.2 7.8 %collective-permute-start.8 = (bf16[16,1536]{1,0:T(8,128)(2,1)S(1)}, bf16[16,1536]{1,0:T(8,128)(2,1)S(1)}, u32[]{:S(2)}, u32[]{:S(2)}) collective-permute-start(bf16[16,1536]{1,0:T(8,128)(2,1)S(1)} %get-tuple-element.38), channel_id=1, source_target_pairs={{0,30},{2,28},{4,26},{6,24},{8,22},{10,20},{12,18},{14,16},{16,14}... | collective-permute-start | bytes 147464 | tf_op jit(solution)/shard_map/ppermute | solution.py:340
  32.7 8.7 %collective-permute-start.14 = (bf16[512,128]{1,0:T(8,128)(2,1)S(1)}, bf16[512,128]{1,0:T(8,128)(2,1)S(1)}, u32[]{:S(2)}, u32[]{:S(2)}) collective-permute-start(bf16[512,128]{1,0:T(8,128)(2,1)S(1)} %copy-done.5), channel_id=1, source_target_pairs={{0,24},{2,26},{4,28},{6,30},{8,16},{10,18},{12,20},{14,22},{16,8},... | collective-permute-start | bytes 393224 | tf_op jit(solution)/shard_map/ppermute | solution.py:340
  37.9 3.9 %collective-permute-start.9 = (bf16[16,896]{1,0:T(8,128)(2,1)S(1)}, bf16[16,896]{1,0:T(8,128)(2,1)S(1)}, u32[]{:S(2)}, u32[]{:S(2)}) collective-permute-start(bf16[16,896]{1,0:T(8,128)(2,1)S(1)} %get-tuple-element.41), channel_id=1, source_target_pairs={{0,2},{2,0},{4,6},{6,4},{8,10},{10,8},{12,14},{14,12},{16,18},{18,... | collective-permute-start | bytes 86024 | tf_op jit(solution)/shard_map/ppermute | solution.py:340
  39.4 3.9 %collective-permute-start.10 = (bf16[16,896]{1,0:T(8,128)(2,1)S(1)}, bf16[16,896]{1,0:T(8,128)(2,1)S(1)}, u32[]{:S(2)}, u32[]{:S(2)}) collective-permute-start(bf16[16,896]{1,0:T(8,128)(2,1)S(1)} %get-tuple-element.42), channel_id=1, source_target_pairs={{0,4},{2,6},{4,0},{6,2},{8,12},{10,14},{12,8},{14,10},{16,20},{18,... | collective-permute-start | bytes 86024 | tf_op jit(solution)/shard_map/ppermute | solution.py:340
  40.9 4.8 %collective-permute-start.11 = (bf16[16,896]{1,0:T(8,128)(2,1)S(1)}, bf16[16,896]{1,0:T(8,128)(2,1)S(1)}, u32[]{:S(2)}, u32[]{:S(2)}) collective-permute-start(bf16[16,896]{1,0:T(8,128)(2,1)S(1)} %get-tuple-element.43), channel_id=1, source_target_pairs={{0,6},{2,4},{4,2},{6,0},{8,14},{10,12},{12,10},{14,8},{16,22},{18,... | collective-permute-start | bytes 86024 | tf_op jit(solution)/shard_map/ppermute | solution.py:340
  45.6 15.6 %copy-start.2 = (bf16[1,1024,2048]{2,1,0:T(8,128)(2,1)S(1)}, bf16[1,1024,2048]{2,1,0:T(8,128)(2,1)}, u32[]{:S(2)}) copy-start(bf16[1,1024,2048]{2,1,0:T(8,128)(2,1)} %down_ref.1) | copy-start | bytes 12582916
  45.9 1.3 %collective-permute-start.15 = (bf16[64,256]{1,0:T(8,128)(2,1)S(1)}, bf16[64,256]{1,0:T(8,128)(2,1)S(1)}, u32[]{:S(2)}, u32[]{:S(2)}) collective-permute-start(bf16[64,256]{1,0:T(8,128)(2,1)S(1)} %get-tuple-element.45), channel_id=1, source_target_pairs={{0,1},{1,0},{2,3},{3,2},{4,5},{5,4},{6,7},{7,6},{8,9},{9,8},{10,11... | collective-permute-start | bytes 98312 | tf_op jit(solution)/shard_map/ppermute | solution.py:343
  47.1 14.1 %copy-start = (bf16[1,2048,1024]{2,1,0:T(8,128)(2,1)S(1)}, bf16[1,2048,1024]{2,1,0:T(8,128)(2,1)}, u32[]{:S(2)}) copy-start(bf16[1,2048,1024]{2,1,0:T(8,128)(2,1)} %gate_ref.1) | copy-start | bytes 12582916
  47.2 14.1 %copy-start.1 = (bf16[1,2048,1024]{2,1,0:T(8,128)(2,1)S(1)}, bf16[1,2048,1024]{2,1,0:T(8,128)(2,1)}, u32[]{:S(2)}) copy-start(bf16[1,2048,1024]{2,1,0:T(8,128)(2,1)} %up_ref.1) | copy-start | bytes 12582916
  47.2 14.1 %copy-start.3 = (f32[2048]{0:T(1024)S(1)}, f32[2048]{0:T(1024)}, u32[]{:S(2)}) copy-start(f32[2048]{0:T(1024)} %param.24) | copy-start | bytes 24580
  59.8 1.4 %collective-permute-start.16 = (bf16[16,24,256]{2,1,0:T(8,128)(2,1)S(1)}, bf16[16,24,256]{2,1,0:T(8,128)(2,1)S(1)}, u32[]{:S(2)}, u32[]{:S(2)}) collective-permute-start(bf16[16,24,256]{2,1,0:T(8,128)(2,1)S(1)} %all_to_all.10.mine_ref), channel_id=1, source_target_pairs={{0,1},{1,0},{2,3},{3,2},{4,5},{5,4},{6,7},{7,6},{8,9},{9,8},{10,11... | collective-permute-start | bytes 589832 | tf_op jit(solution)/shard_map/ppermute | solution.py:343
  64.3 1.5 %collective-permute-start.17 = (bf16[384,256]{1,0:T(8,128)(2,1)S(1)}, bf16[384,256]{1,0:T(8,128)(2,1)S(1)}, u32[]{:S(2)}, u32[]{:S(2)}) collective-permute-start(bf16[384,256]{1,0:T(8,128)(2,1)S(1)} %get-tuple-element.50), channel_id=1, source_target_pairs={{0,1},{1,0},{2,3},{3,2},{4,5},{5,4},{6,7},{7,6},{8,9},{9,8},{10,11... | collective-permute-start | bytes 589832 | tf_op jit(solution)/shard_map/ppermute | solution.py:343
  66.6 12.4 %all-to-all-start.1 = ((bf16[16,24,256]{2,1,0:T(8,128)(2,1)}), bf16[16,24,256]{2,1,0:T(8,128)(2,1)S(1)}, u32[]{:S(2)}, u32[]{:S(2)}) async-start(bf16[16,24,256]{2,1,0:T(8,128)(2,1)} %bitcast.4), calls=%async_computation.1 | async-start | bytes 393216 | tf_op jit(solution)/shard_map/all_to_all | solution.py:419
  70.1 8.8 %collective-permute-start.18 = (bf16[16,256]{1,0:T(8,128)(2,1)S(1)}, bf16[16,256]{1,0:T(8,128)(2,1)S(1)}, u32[]{:S(2)}, u32[]{:S(2)}) collective-permute-start(bf16[16,256]{1,0:T(8,128)(2,1)S(1)} %get-tuple-element.53), channel_id=1, source_target_pairs={{0,2},{2,0},{4,6},{6,4},{8,10},{10,8},{12,14},{14,12},{16,18},{18,... | collective-permute-start | bytes 24584 | tf_op jit(solution)/shard_map/ppermute | solution.py:340
  71.9 7.0 %collective-permute-start.19 = (bf16[16,256]{1,0:T(8,128)(2,1)S(1)}, bf16[16,256]{1,0:T(8,128)(2,1)S(1)}, u32[]{:S(2)}, u32[]{:S(2)}) collective-permute-start(bf16[16,256]{1,0:T(8,128)(2,1)S(1)} %get-tuple-element.54), channel_id=1, source_target_pairs={{0,4},{2,6},{4,0},{6,2},{8,12},{10,14},{12,8},{14,10},{16,20},{18,... | collective-permute-start | bytes 24584 | tf_op jit(solution)/shard_map/ppermute | solution.py:340
  73.4 5.5 %collective-permute-start.20 = (bf16[16,256]{1,0:T(8,128)(2,1)S(1)}, bf16[16,256]{1,0:T(8,128)(2,1)S(1)}, u32[]{:S(2)}, u32[]{:S(2)}) collective-permute-start(bf16[16,256]{1,0:T(8,128)(2,1)S(1)} %get-tuple-element.55), channel_id=1, source_target_pairs={{0,6},{2,4},{4,2},{6,0},{8,14},{10,12},{12,10},{14,8},{16,22},{18,... | collective-permute-start | bytes 24584 | tf_op jit(solution)/shard_map/ppermute | solution.py:340

commit v3 on v2

--- a/solution.py
+++ b/solution.py
@@ -187,12 +187,23 @@
         out[:, proj + half * LANES :] = info_ref[...]
 
 
-def update_kernel(forget_ref, fresh_ref, state_ref, new_ref):
+def update_kernel(forget_ref, fresh_ref, state_ref, new_ref, slot_ref, sems):
     count = forget_ref.shape[0]
-    kept = spread(forget_ref[...], spreader(count))
-    for s in range(count):
-        keep = kept[:, s * LANES : (s + 1) * LANES]
-        new_ref[s, 0] = keep * state_ref[s, 0] + (1.0 - keep) * fresh_ref[s : s + 1, :]
+    heads = state_ref.shape[1]
+    matrix = spreader(count)
+    copies = []
+    for head in range(heads):
+        cols = slice(head * LANES, (head + 1) * LANES)
+        kept = spread(forget_ref[:, cols], matrix)
+        fresh = fresh_ref[:, cols]
+        for s in range(count):
+            keep = kept[:, s * LANES : (s + 1) * LANES]
+            slot_ref[head, s] = keep * state_ref[s, head] + (1.0 - keep) * fresh[s : s + 1, :]
+        copy = pltpu.make_async_copy(slot_ref.at[head], new_ref.at[:, head], sems.at[head])
+        copy.start()
+        copies.append(copy)
+    for copy in copies:
+        copy.wait()
 
 
 def mix_kernel(outer, *refs):
@@ -244,43 +255,73 @@
             out_ref[e * span + sp] = picked
 
 
-def expert_kernel(outer, mine_ref, theirs_ref, gain_ref, gate_ref, up_ref, down_ref, own_ref, other_ref, rows_ref, total_ref):
-    core = lax.axis_index("tp")
+def gather_rows(outer, ref, rows_ref):
     half = outer // 2
-    total_rows, width = rows_ref.shape[0], rows_ref.shape[1] // 2
-    block = mine_ref.shape[1]
-    cap = block // GROUP
-    for ref, side in ((mine_ref, core), (theirs_ref, 1 - core)):
-        for z in range(outer):
-            for q in range(GROUP):
-                for a in range(half):
-                    at = side * width + (a * GROUP + q) * LANES
-                    rows_ref[z * block : (z + 1) * block, aligned(at, LANES)] = ref[
-                        z * GROUP + q, :, a * LANES : (a + 1) * LANES
-                    ].astype(jnp.float32)
-    values = rows_ref[...]
-    scale = lax.rsqrt(jnp.mean(values * values, axis=-1, keepdims=True) + epsilon)
-    rows = (values * scale * gain_ref[...]).astype(jnp.bfloat16)
-    gate = jnp.dot(rows, gate_ref[0], preferred_element_type=jnp.float32)
-    up = jnp.dot(rows, up_ref[0], preferred_element_type=jnp.float32)
-    hidden = (jax.nn.silu(gate) * up).astype(jnp.bfloat16)
-    total_ref[...] = jnp.dot(hidden, down_ref[0], preferred_element_type=jnp.float32).astype(jnp.bfloat16)
-    part = width // GROUP
-    tall = own_ref.shape[0]
-    row = lax.broadcasted_iota(jnp.int32, (tall, total_rows), 0)
-    col = lax.broadcasted_iota(jnp.int32, (tall, total_rows), 1)
+    block = ref.shape[1]
+    for z in range(outer):
+        for q in range(GROUP):
+            for a in range(half):
+                at = (a * GROUP + q) * LANES
+                rows_ref[z * block : (z + 1) * block, at : at + LANES] = ref[
+                    z * GROUP + q, :, a * LANES : (a + 1) * LANES
+                ].astype(jnp.float32)
+    return rows_ref[...]
+
+
+def half_products(outer, side, ref, gain_ref, gate_ref, up_ref, rows_ref):
+    width = rows_ref.shape[1]
+    at = aligned(side * width, width)
+    values = gather_rows(outer, ref, rows_ref)
+    square = jnp.sum(values * values, axis=-1, keepdims=True)
+    scaled = (values * gain_ref[:, at]).astype(jnp.bfloat16)
+    gate = jnp.dot(scaled, gate_ref[0, at, :], preferred_element_type=jnp.float32)
+    up = jnp.dot(scaled, up_ref[0, at, :], preferred_element_type=jnp.float32)
+    return square, gate, up
+
+
+def first_kernel(outer, mine_ref, gain_ref, gate_ref, up_ref, square_ref, gate_out, up_out, rows_ref):
+    side = lax.axis_index("tp")
+    square, gate, up = half_products(outer, side, mine_ref, gain_ref, gate_ref, up_ref, rows_ref)
+    square_ref[...] = jnp.broadcast_to(square, square_ref.shape)
+    gate_out[...] = gate
+    up_out[...] = up
+
+
+def pack_half(side, hidden, down_ref, out_ref, block, cap):
+    part = out_ref.shape[1]
+    width = part * GROUP
+    total = jnp.dot(
+        hidden, down_ref[0, :, aligned(side * width, width)], preferred_element_type=jnp.float32
+    ).astype(jnp.bfloat16)
+    shape = (out_ref.shape[0], total.shape[0])
+    row = lax.broadcasted_iota(jnp.int32, shape, 0)
     source = (row // block) * cap + row % cap
     piece = (row % block) // cap
-    selects = [
-        jnp.where((source == col) & (piece == k), 1.0, 0.0).astype(jnp.bfloat16) for k in range(GROUP)
-    ]
-    for ref, side in ((other_ref, 1 - core), (own_ref, core)):
-        packed = None
-        for k, select in enumerate(selects):
-            values = total_ref[:, aligned(side * width + k * part, part)]
-            term = jnp.dot(select, values, preferred_element_type=jnp.float32)
-            packed = term if packed is None else packed + term
-        ref[...] = packed.astype(jnp.bfloat16)
+    here = source == lax.broadcasted_iota(jnp.int32, shape, 1)
+    packed = None
+    for k in range(GROUP):
+        select = jnp.where(here & (piece == k), 1.0, 0.0).astype(jnp.bfloat16)
+        term = jnp.dot(
+            select, total[:, k * part : (k + 1) * part], preferred_element_type=jnp.float32
+        )
+        packed = term if packed is None else packed + term
+    out_ref[...] = packed.astype(jnp.bfloat16)
+
+
+def second_kernel(outer, cap, theirs_ref, gain_ref, gate_ref, up_ref, down_ref, square_ref, gate_part, up_part, hidden_ref, other_ref, rows_ref):
+    side = 1 - lax.axis_index("tp")
+    width = 2 * rows_ref.shape[1]
+    square, gate, up = half_products(outer, side, theirs_ref, gain_ref, gate_ref, up_ref, rows_ref)
+    scale = lax.rsqrt((square_ref[:, :1] + square) / width + epsilon)
+    gate = (gate_part[...] + gate) * scale
+    up = (up_part[...] + up) * scale
+    hidden = (jax.nn.silu(gate) * up).astype(jnp.bfloat16)
+    hidden_ref[...] = hidden
+    pack_half(side, hidden, down_ref, other_ref, GROUP * cap, cap)
+
+
+def third_kernel(cap, hidden_ref, down_ref, own_ref):
+    pack_half(lax.axis_index("tp"), hidden_ref[...], down_ref, own_ref, GROUP * cap, cap)
 
 
 def combine_kernel(outer, cap, got_ref, weight_ref, *refs):
@@ -386,6 +427,19 @@
         [shaped(count, proj, dtype=f32)] * 2 + [shaped(count, pay)] * GROUP,
     )
     payloads = [move(value, m) for m, value in enumerate(payloads)]
+    vmem = pl.BlockSpec(memory_space=pltpu.VMEM)
+    new_state = pl.pallas_call(
+        update_kernel,
+        out_shape=shaped(*state.shape, dtype=f32),
+        in_specs=[vmem] * 3,
+        out_specs=pl.BlockSpec(memory_space=pltpu.HBM),
+        scratch_shapes=[
+            pltpu.VMEM((heads, count, size, size), f32),
+            pltpu.SemaphoreType.DMA((heads,)),
+        ],
+        compiler_params=pltpu.CompilerParams(vmem_limit_bytes=12 << 20),
+        cost_estimate=pl.CostEstimate(flops=1_000_000_000, bytes_accessed=100_000, transcendentals=0),
+    )(forget, fresh, state)
 
     tall = GROUP * count
     own, other, resid, infos = call(
@@ -408,28 +462,35 @@
     total_rows = ep * cap
     tall = ep * rows_out
     part = width // 2 // GROUP
-    mine, theirs = call(
-        functools.partial(expert_kernel, outer),
-        (slot_rows, other_rows, ffn_gain.reshape(1, width), expert_gate, expert_up, expert_down),
-        [shaped(tall, part)] * 2,
-        scratch=[pltpu.VMEM((total_rows, width), f32), pltpu.VMEM((total_rows, width), bf16)],
-        mib=24,
-    )
-    reduced = (mine.astype(f32) + swap(theirs).astype(f32)).astype(bf16)
+    wide = expert_gate.shape[2]
+    gain = ffn_gain.reshape(1, width)
+    rows_scratch = [pltpu.VMEM((total_rows, width // 2), f32)]
+    square, gate_part, up_part = call(
+        functools.partial(first_kernel, outer),
+        (slot_rows, gain, expert_gate, expert_up),
+        [shaped(total_rows, LANES, dtype=f32)] + [shaped(total_rows, wide, dtype=f32)] * 2,
+        scratch=rows_scratch,
+        mib=14,
+        flops=100_000_000,
+    )
+    hidden, theirs = call(
+        functools.partial(second_kernel, outer, cap),
+        (other_rows, gain, expert_gate, expert_up, expert_down, square, gate_part, up_part),
+        [shaped(total_rows, wide), shaped(tall, part)],
+        scratch=rows_scratch,
+        mib=20,
+    )
+    theirs = swap(theirs)
+    mine = call(
+        functools.partial(third_kernel, cap),
+        (hidden, expert_down),
+        [shaped(tall, part)],
+        mib=10,
+    )[0]
+    reduced = (mine.astype(f32) + theirs.astype(f32)).astype(bf16)
     returned = lax.all_to_all(
         reduced.reshape(ep, rows_out, part), "ep", split_axis=0, concat_axis=0, tiled=True
     )
-    block = pl.BlockSpec((count, 1, size, size), lambda h: (0, h, 0, 0))
-    column = pl.BlockSpec((count, size), lambda h: (0, h))
-    new_state = pl.pallas_call(
-        update_kernel,
-        out_shape=shaped(*state.shape, dtype=f32),
-        grid=(heads,),
-        in_specs=[column, column, block],
-        out_specs=block,
-        compiler_params=pltpu.CompilerParams(vmem_limit_bytes=12 << 20),
-        cost_estimate=pl.CostEstimate(flops=3_000_000_000, bytes_accessed=8_000_000, transcendentals=0),
-    )(forget, fresh, pltpu.with_memory_space_constraint(state, pltpu.HBM))
     mixed_out = call(
         functools.partial(combine_kernel, outer, cap),
         (returned.reshape(tall, part), combine, *afters),

time: 80.2 us -> 79.8 us (level)
  local copies, waits for them, and re-layouts: 0.21 us -> 3.17 us
  Pallas kernels: 12.5 us -> 10 us
  waiting for transfers between devices: 20 us -> 18.7 us
    unnamed x26 -> x28, local copies, waits for them, and re-layouts: 0.21 us -> 3.17 us
    pallas_call x1, Pallas kernels: 5.24 us -> 2.37 us  [fast_shards(): pl.pallas_call(update_kernel, out_shape=shaped(*state.shape, dtype=f32),...]
    ppermute x3, waiting for transfers between devices: 3.94 us -> 1.91 us  [swap(): return lax.ppermute(value, 'tp', [(0, 1), (1, 0)])]
    pallas_call x8 -> x10, Pallas kernels: 7.24 us -> 7.66 us  [call(): pl.pallas_call(kernel, out_shape=outs, in_specs=[pl.BlockSpec(memory_spac...]
  transfers between devices with their start and end apart: 22 -> 22, of which waited for: 10 -> 10; matrix products, arithmetic and copies ran while one was open for 0% -> 0% of each run, Pallas kernels for 9% -> 7%
where the time goes in v3:
time: 79.8 us; the launch traced here: 79.5 us
  starting transfers between devices  33.6 us (42%)
  waiting for transfers between devices  18.7 us (23%)
  blocking collectives  12.4 us (16%)
  Pallas kernels  10 us (13%)
  local copies, waits for them, and re-layouts  3.17 us (4%)
  between operations  0.85 us (1%)
    ppermute x18, starting transfers between devices, move(): return lax.ppermute(value, 'ep', xor_pairs(ep, mask))  29.5 us
    ppermute x18, waiting for transfers between devices, move(): return lax.ppermute(value, 'ep', xor_pairs(ep, mask))  15.9 us
    all_to_all x1, blocking collectives, fast_shards(): lax.all_to_all(outgoing, 'ep', split_axis=0, concat_axis=0, tiled=True)  12.4 us
    pallas_call x10, Pallas kernels, call(): pl.pallas_call(kernel, out_shape=outs, in_specs=[pl.BlockSpec(memory_spac...  7.66 us
    all_to_all x1, starting transfers between devices, fast_shards(): lax.all_to_all(reduced.reshape(ep, rows_out, part), 'ep', split_axis=0, c...  3.52 us
    unnamed x28, local copies, waits for them, and re-layouts  3.17 us
    pallas_call x1, Pallas kernels, fast_shards(): pl.pallas_call(update_kernel, out_shape=shaped(*state.shape, dtype=f32),...  2.37 us
    ppermute x3, waiting for transfers between devices, swap(): return lax.ppermute(value, 'tp', [(0, 1), (1, 0)])  1.91 us
  transfers between devices with their start and end apart: 22, of which 10 were waited for; matrix products, arithmetic and copies ran while one was open for 0% of the time, Pallas kernels for 7%

profile of v3, /device:TPU:0, one launch (start us, length us, event | category | flops | bytes accessed | tf_op | source)
XLA Modules:
  0.0 79.5 jit_solution(13427576452208798116)
XLA Ops:
  0.6 0.0 copy-start.11
  0.6 0.0 copy-start.12
  0.7 1.3 %shard_map.158 = (bf16[128,1536]{1,0:T(8,128)(2,1)S(1)}, bf16[16,512]{1,0:T(8,128)(2,1)S(1)}, bf16[16,512]{1,0:T(8,128)(2,1)S(1)}, bf16[16,512]{1,0:T(8,128)(2,1)S(1)}, bf16[16,512]{1,0:T(8,128)(2,1)S(1)}) custom-call(bf16[16,2048]{1,0:T(8,128)(2,1)} %refs_4_.2, bf16[128,512]{1,0:T(8,128)(2,1)} %refs_0_.1, bf16[128,512]{1,0:T(8,128)(2,1)} %refs_1_.1, ...), custom_call_target="tpu_custom_call" | custom-call | flops 3000000000 | bytes 100000 | tf_op jit(solution)/shard_map/pallas_call | solution.py:32
  1.9 3.1 %collective-permute-start.5 = (bf16[128,1536]{1,0:T(8,128)(2,1)S(1)}, bf16[128,1536]{1,0:T(8,128)(2,1)S(1)}, u32[]{:S(2)}, u32[]{:S(2)}) collective-permute-start(bf16[128,1536]{1,0:T(8,128)(2,1)S(1)} %get-tuple-element.37.refs_5_), channel_id=1, source_target_pairs={{0,8},{2,10},{4,12},{6,14},{8,0},{10,2},{12,4},{14,6},{16,24},{18,... | collective-permute-start | bytes 1179656 | tf_op jit(solution)/shard_map/ppermute | solution.py:381
  5.1 1.5 %collective-permute-start.4 = (bf16[128,1536]{1,0:T(8,128)(2,1)S(1)}, bf16[128,1536]{1,0:T(8,128)(2,1)S(1)}, u32[]{:S(2)}, u32[]{:S(2)}) collective-permute-start(bf16[128,1536]{1,0:T(8,128)(2,1)S(1)} %get-tuple-element.37.refs_5_), channel_id=1, source_target_pairs={{0,4},{2,6},{4,0},{6,2},{8,12},{10,14},{12,8},{14,10},{16,20},{18,... | collective-permute-start | bytes 1179656 | tf_op jit(solution)/shard_map/ppermute | solution.py:381
  6.6 1.5 %collective-permute-start.3 = (bf16[128,1536]{1,0:T(8,128)(2,1)S(1)}, bf16[128,1536]{1,0:T(8,128)(2,1)S(1)}, u32[]{:S(2)}, u32[]{:S(2)}) collective-permute-start(bf16[128,1536]{1,0:T(8,128)(2,1)S(1)} %get-tuple-element.37.refs_5_), channel_id=1, source_target_pairs={{0,2},{2,0},{4,6},{6,4},{8,10},{10,8},{12,14},{14,12},{16,18},{18,... | collective-permute-start | bytes 1179656 | tf_op jit(solution)/shard_map/ppermute | solution.py:381
  8.1 0.0 collective-permute-start
  8.1 2.9 %collective-permute-start.1 = (bf16[16,512]{1,0:T(8,128)(2,1)S(1)}, bf16[16,512]{1,0:T(8,128)(2,1)S(1)}, u32[]{:S(2)}, u32[]{:S(2)}) collective-permute-start(bf16[16,512]{1,0:T(8,128)(2,1)S(1)} %get-tuple-element.35), channel_id=1, source_target_pairs={{0,16},{2,18},{4,20},{6,22},{8,24},{10,26},{12,28},{14,30},{16,0},... | collective-permute-start | bytes 49160 | tf_op jit(solution)/shard_map/ppermute | solution.py:381
  11.0 6.0 %collective-permute-done.refs_1_ = bf16[16,512]{1,0:T(8,128)(2,1)S(1)} collective-permute-done((bf16[16,512]{1,0:T(8,128)(2,1)S(1)}, bf16[16,512]{1,0:T(8,128)(2,1)S(1)}, u32[]{:S(2)}, u32[]{:S(2)}) %collective-permute-start) | collective-permute-done | bytes 16416 | tf_op jit(solution)/shard_map/ppermute | solution.py:381
  17.0 3.5 %collective-permute-start.2 = (bf16[16,512]{1,0:T(8,128)(2,1)S(1)}, bf16[16,512]{1,0:T(8,128)(2,1)S(1)}, u32[]{:S(2)}, u32[]{:S(2)}) collective-permute-start(bf16[16,512]{1,0:T(8,128)(2,1)S(1)} %get-tuple-element.36), channel_id=1, source_target_pairs={{0,30},{2,28},{4,26},{6,24},{8,22},{10,20},{12,18},{14,16},{16,14}... | collective-permute-start | bytes 49160 | tf_op jit(solution)/shard_map/ppermute | solution.py:381
  20.6 0.1 copy.17.ids_ref
  20.6 0.1 copy.18.weights_ref
  20.7 0.0 collective-permute-done.1.refs_2_
  20.7 0.0 collective-permute-start.13
  20.8 3.9 %collective-permute-done.2.refs_3_ = bf16[16,512]{1,0:T(8,128)(2,1)S(1)} collective-permute-done((bf16[16,512]{1,0:T(8,128)(2,1)S(1)}, bf16[16,512]{1,0:T(8,128)(2,1)S(1)}, u32[]{:S(2)}, u32[]{:S(2)}) %collective-permute-start.2) | collective-permute-done | bytes 16416 | tf_op jit(solution)/shard_map/ppermute | solution.py:381
  24.6 0.8 %collective-permute-start.12 = (bf16[512,128]{1,0:T(8,128)(2,1)S(1)}, bf16[512,128]{1,0:T(8,128)(2,1)S(1)}, u32[]{:S(2)}, u32[]{:S(2)}) collective-permute-start(bf16[512,128]{1,0:T(8,128)(2,1)S(1)} %copy-done.6), channel_id=1, source_target_pairs={{0,8},{2,10},{4,12},{6,14},{8,0},{10,2},{12,4},{14,6},{16,24},{18,... | collective-permute-start | bytes 393224 | tf_op jit(solution)/shard_map/ppermute | solution.py:381
  25.5 0.0 collective-permute-done.5.refs_8_
  25.5 0.0 collective-permute-done.4.refs_7_
  25.5 0.0 collective-permute-done.3.refs_6_
  25.5 0.4 shard_map.159
  25.9 1.0 %collective-permute-start.6 = (bf16[16,1536]{1,0:T(8,128)(2,1)S(1)}, bf16[16,1536]{1,0:T(8,128)(2,1)S(1)}, u32[]{:S(2)}, u32[]{:S(2)}) collective-permute-start(bf16[16,1536]{1,0:T(8,128)(2,1)S(1)} %get-tuple-element.39), channel_id=1, source_target_pairs={{0,14},{2,12},{4,10},{6,8},{8,6},{10,4},{12,2},{14,0},{16,30},{18,... | collective-permute-start | bytes 147464 | tf_op jit(solution)/shard_map/ppermute | solution.py:381
  26.9 2.3 %collective-permute-start.7 = (bf16[16,1536]{1,0:T(8,128)(2,1)S(1)}, bf16[16,1536]{1,0:T(8,128)(2,1)S(1)}, u32[]{:S(2)}, u32[]{:S(2)}) collective-permute-start(bf16[16,1536]{1,0:T(8,128)(2,1)S(1)} %get-tuple-element.40), channel_id=1, source_target_pairs={{0,16},{2,18},{4,20},{6,22},{8,24},{10,26},{12,28},{14,30},{16,0},... | collective-permute-start | bytes 147464 | tf_op jit(solution)/shard_map/ppermute | solution.py:381
  29.2 3.3 %collective-permute-start.8 = (bf16[16,1536]{1,0:T(8,128)(2,1)S(1)}, bf16[16,1536]{1,0:T(8,128)(2,1)S(1)}, u32[]{:S(2)}, u32[]{:S(2)}) collective-permute-start(bf16[16,1536]{1,0:T(8,128)(2,1)S(1)} %get-tuple-element.41), channel_id=1, source_target_pairs={{0,30},{2,28},{4,26},{6,24},{8,22},{10,20},{12,18},{14,16},{16,14}... | collective-permute-start | bytes 147464 | tf_op jit(solution)/shard_map/ppermute | solution.py:381
  32.4 0.3 shard_map.160
  32.7 0.0 collective-permute-done.6.refs_1_
  32.7 2.4 %collective-permute-start.14 = (bf16[512,128]{1,0:T(8,128)(2,1)S(1)}, bf16[512,128]{1,0:T(8,128)(2,1)S(1)}, u32[]{:S(2)}, u32[]{:S(2)}) collective-permute-start(bf16[512,128]{1,0:T(8,128)(2,1)S(1)} %copy-done.6), channel_id=1, source_target_pairs={{0,24},{2,26},{4,28},{6,30},{8,16},{10,18},{12,20},{14,22},{16,8},... | collective-permute-start | bytes 393224 | tf_op jit(solution)/shard_map/ppermute | solution.py:381
  35.1 0.0 collective-permute-done.7.refs_2_
  35.1 1.8 %collective-permute-done.8.refs_3_ = bf16[16,1536]{1,0:T(8,128)(2,1)S(1)} collective-permute-done((bf16[16,1536]{1,0:T(8,128)(2,1)S(1)}, bf16[16,1536]{1,0:T(8,128)(2,1)S(1)}, u32[]{:S(2)}, u32[]{:S(2)}) %collective-permute-start.8) | collective-permute-done | bytes 49184 | tf_op jit(solution)/shard_map/ppermute | solution.py:381
  37.0 1.0 %shard_map.161 = (f32[16,512]{1,0:T(8,128)S(1)}, f32[16,512]{1,0:T(8,128)S(1)}, bf16[16,896]{1,0:T(8,128)(2,1)S(1)}, bf16[16,896]{1,0:T(8,128)(2,1)S(1)}, bf16[1...) custom-call(bf16[16,1536]{1,0:T(8,128)(2,1)S(1)} %get-tuple-element.38.refs_0_, ...), custom_call_target="tpu_custom_call" | custom-call | flops 3000000000 | bytes 100000 | tf_op jit(solution)/shard_map/pallas_call | solution.py:32
  37.9 1.4 %collective-permute-start.9 = (bf16[16,896]{1,0:T(8,128)(2,1)S(1)}, bf16[16,896]{1,0:T(8,128)(2,1)S(1)}, u32[]{:S(2)}, u32[]{:S(2)}) collective-permute-start(bf16[16,896]{1,0:T(8,128)(2,1)S(1)} %get-tuple-element.44), channel_id=1, source_target_pairs={{0,2},{2,0},{4,6},{6,4},{8,10},{10,8},{12,14},{14,12},{16,18},{18,... | collective-permute-start | bytes 86024 | tf_op jit(solution)/shard_map/ppermute | solution.py:381
  39.4 1.5 %collective-permute-start.10 = (bf16[16,896]{1,0:T(8,128)(2,1)S(1)}, bf16[16,896]{1,0:T(8,128)(2,1)S(1)}, u32[]{:S(2)}, u32[]{:S(2)}) collective-permute-start(bf16[16,896]{1,0:T(8,128)(2,1)S(1)} %get-tuple-element.45), channel_id=1, source_target_pairs={{0,4},{2,6},{4,0},{6,2},{8,12},{10,14},{12,8},{14,10},{16,20},{18,... | collective-permute-start | bytes 86024 | tf_op jit(solution)/shard_map/ppermute | solution.py:381
  40.9 0.0 collective-permute-done.13.refs_6_
  40.9 0.6 collective-permute-start.11
  41.4 0.0 collective-permute-done.12.refs_5_
  41.4 0.0 collective-permute-done.14.refs_7_
  41.4 0.4 collective-permute-done.9.refs_1_
  41.8 1.4 %collective-permute-done.10.refs_2_ = bf16[16,896]{1,0:T(8,128)(2,1)S(1)} collective-permute-done((bf16[16,896]{1,0:T(8,128)(2,1)S(1)}, bf16[16,896]{1,0:T(8,128)(2,1)S(1)}, u32[]{:S(2)}, u32[]{:S(2)}) %collective-permute-start.10) | collective-permute-done | bytes 28704 | tf_op jit(solution)/shard_map/ppermute | solution.py:381
  43.2 2.4 %collective-permute-done.11.refs_3_ = bf16[16,896]{1,0:T(8,128)(2,1)S(1)} collective-permute-done((bf16[16,896]{1,0:T(8,128)(2,1)S(1)}, bf16[16,896]{1,0:T(8,128)(2,1)S(1)}, u32[]{:S(2)}, u32[]{:S(2)}) %collective-permute-start.11) | collective-permute-done | bytes 28704 | tf_op jit(solution)/shard_map/ppermute | solution.py:381
  45.6 0.2 shard_map.162
  45.9 0.1 collective-permute-start.15
  45.9 1.2 %collective-permute-done.15.got_ref = bf16[64,256]{1,0:T(8,128)(2,1)S(1)} collective-permute-done((bf16[64,256]{1,0:T(8,128)(2,1)S(1)}, bf16[64,256]{1,0:T(8,128)(2,1)S(1)}, u32[]{:S(2)}, u32[]{:S(2)}) %collective-permute-start.15) | collective-permute-done | bytes 32800 | tf_op jit(solution)/shard_map/ppermute | solution.py:384
  47.1 0.2 shard_map.163
  47.4 12.4 %all_to_all.10.mine_ref = bf16[16,24,256]{2,1,0:T(8,128)(2,1)S(1)} all-to-all(bf16[16,24,256]{2,1,0:T(8,128)(2,1)S(1)} %get-tuple-element.51), channel_id=1, replica_groups=mesh['ep'=16,'tp'=2] {'ep'}, dimensions={0} | all-to-all | bytes 393216 | tf_op jit(solution)/shard_map/all_to_all | solution.py:458
  59.8 0.0 collective-permute-start.16
  59.8 0.0 copy-start.2
  59.8 0.8 %shard_map.164 = (f32[96,128]{1,0:T(8,128)S(1)}, f32[96,1024]{1,0:T(8,128)S(1)}, f32[96,1024]{1,0:T(8,128)S(1)}) custom-call(bf16[16,24,256]{2,1,0:T(8,128)(2,1)S(1)} %all_to_all.10.mine_ref, f32[1,2048]{1,0:T(1,128)S(1)} %bitcast.7, bf16[1,2048,1024]{2,1,0:T(8,128)(2,1)S(1)} %copy-done, bf16[1,2048,1024]{2,1,0:T(8,128)(2,1)S(1)} %copy-done.1), custom_call_target="tpu_custom_call" | custom-call | flops 100000000 | bytes 100000 | tf_op jit(solution)/shard_map/pallas_call | solution.py:32
  60.7 0.6 collective-permute-done.16.theirs_ref
  61.3 0.8 copy-done.2
  62.0 1.7 %shard_map.165 = (bf16[96,1024]{1,0:T(8,128)(2,1)S(1)}, bf16[384,256]{1,0:T(8,128)(2,1)S(1)}) custom-call(bf16[16,24,256]{2,1,0:T(8,128)(2,1)S(1)} %collective-permute-done.16.theirs_ref, f32[1,2048]{1,0:T(1,128)S(1)} %bitcast.8, bf16[1,2048,1024]{2,1,0:T(8,128)(2,1)S(1)} %copy-done, bf16[1,2048,1024]{2,1,0:T(8,128)(2,1)S(1)} %copy-done.1, ...), custom_call_target="tpu_custom_call" | custom-call | flops 3000000000 | bytes 100000 | tf_op jit(solution)/shard_map/pallas_call | solution.py:32
  63.8 0.6 collective-permute-start.17
  64.3 0.9 %shard_map.166 = bf16[384,256]{1,0:T(8,128)(2,1)S(1)} custom-call(bf16[96,1024]{1,0:T(8,128)(2,1)S(1)} %get-tuple-element.55.hidden_ref, bf16[1,1024,2048]{2,1,0:T(8,128)(2,1)S(1)} %copy-done.2), custom_call_target="tpu_custom_call" | custom-call | flops 3000000000 | bytes 100000 | tf_op jit(solution)/shard_map/pallas_call | solution.py:32
  65.3 0.1 collective-permute-done.17
  65.4 0.7 add_convert_fusion
  66.1 3.5 %all-to-all-start.1 = ((bf16[16,24,256]{2,1,0:T(8,128)(2,1)}), bf16[16,24,256]{2,1,0:T(8,128)(2,1)S(1)}, u32[]{:S(2)}, u32[]{:S(2)}) async-start(bf16[16,24,256]{2,1,0:T(8,128)(2,1)} %bitcast.4), calls=%async_computation.1 | async-start | bytes 393216 | tf_op jit(solution)/shard_map/all_to_all | solution.py:491
  69.6 1.8 %collective-permute-start.18 = (bf16[16,256]{1,0:T(8,128)(2,1)S(1)}, bf16[16,256]{1,0:T(8,128)(2,1)S(1)}, u32[]{:S(2)}, u32[]{:S(2)}) collective-permute-start(bf16[16,256]{1,0:T(8,128)(2,1)S(1)} %get-tuple-element.59), channel_id=1, source_target_pairs={{0,2},{2,0},{4,6},{6,4},{8,10},{10,8},{12,14},{14,12},{16,18},{18,... | collective-permute-start | bytes 24584 | tf_op jit(solution)/shard_map/ppermute | solution.py:381
  71.4 1.5 %collective-permute-start.19 = (bf16[16,256]{1,0:T(8,128)(2,1)S(1)}, bf16[16,256]{1,0:T(8,128)(2,1)S(1)}, u32[]{:S(2)}, u32[]{:S(2)}) collective-permute-start(bf16[16,256]{1,0:T(8,128)(2,1)S(1)} %get-tuple-element.60), channel_id=1, source_target_pairs={{0,4},{2,6},{4,0},{6,2},{8,12},{10,14},{12,8},{14,10},{16,20},{18,... | collective-permute-start | bytes 24584 | tf_op jit(solution)/shard_map/ppermute | solution.py:381
  72.9 0.3 collective-permute-start.20
  73.2 2.2 %copy-done.4 = f32[16,4,128,128]{3,2,1,0:T(8,128)S(1)} copy-done((f32[16,4,128,128]{3,2,1,0:T(8,128)S(1)}, f32[16,4,128,128]{3,2,1,0:T(8,128)}, u32[]{:S(2)}) %copy-start.4) | copy-done | bytes 4194328
  75.4 2.4 %shard_map.168 = f32[16,4,128,128]{3,2,1,0:T(8,128)} custom-call(f32[16,512]{1,0:T(8,128)S(1)} %get-tuple-element.62.forget_ref, f32[16,512]{1,0:T(8,128)S(1)} %get-tuple-element.63.fresh_ref, f32[16,4,128,128]{3,2,1,0:T(8,128)S(1)} %copy-done.4), custom_call_target="tpu_custom_call" | custom-call | flops 1000000000 | bytes 100000 | tf_op jit(solution)/shard_map/pallas_call | solution.py:431
  77.8 0.0 collective-permute-done.18.refs_1_
  77.8 0.0 collective-permute-done.19.refs_2_
  77.8 0.0 collective-permute-done.20.refs_3_
  77.8 0.8 %all-to-all-done.1 = bf16[16,24,256]{2,1,0:T(8,128)(2,1)S(1)} async-done(((bf16[16,24,256]{2,1,0:T(8,128)(2,1)}), bf16[16,24,256]{2,1,0:T(8,128)(2,1)S(1)}, u32[]{:S(2)}, u32[]{:S(2)}) %all-to-all-start.1) | async-done | bytes 196640 | tf_op jit(solution)/shard_map/all_to_all | solution.py:491
  78.6 0.9 %shard_map.167 = bf16[16,1024]{1,0:T(8,128)(2,1)} custom-call(bf16[384,256]{1,0:T(8,128)(2,1)S(1)} %bitcast.6, f32[16,384]{1,0:T(8,128)S(1)} %get-tuple-element.57.weight_ref, bf16[16,256]{1,0:T(8,128)(2,1)S(1)} %get-tuple-element.58.refs_0_, bf16[16,256]{1,0:T(8,128)(2,1)S(1)} %collective-permute-done.18.refs_1_, ...), custom_call_target="tpu_custom_call" | custom-call | flops 3000000000 | bytes 100000 | tf_op jit(solution)/shard_map/pallas_call | solution.py:32
  (21 shorter events, 0.0 us)
Async XLA Ops:
  0.6 19.9 %copy-start.11 = (s32[16,2]{0,1:T(2,128)S(1)}, s32[16,2]{0,1:T(2,128)}, u32[]{:S(2)}) copy-start(s32[16,2]{0,1:T(2,128)} %param.25) | copy-start | bytes 388
  0.6 20.0 %copy-start.12 = (f32[16,2]{0,1:T(2,128)S(1)}, f32[16,2]{0,1:T(2,128)}, u32[]{:S(2)}) copy-start(f32[16,2]{0,1:T(2,128)} %param.26) | copy-start | bytes 388
  0.7 20.1 %copy-start.6 = (bf16[512,128]{1,0:T(8,128)(2,1)S(1)}, bf16[512,128]{1,0:T(8,128)(2,1)}, u32[]{:S(2)}) copy-start(bf16[512,128]{1,0:T(8,128)(2,1)} %refs_4_.3) | copy-start | bytes 393220
  0.7 24.8 %copy-start.8 = (f32[2048]{0:T(1024)S(1)}, f32[2048]{0:T(1024)}, u32[]{:S(2)}) copy-start(f32[2048]{0:T(1024)} %param.16) | copy-start | bytes 24580
  1.9 23.5 %collective-permute-start.5 = (bf16[128,1536]{1,0:T(8,128)(2,1)S(1)}, bf16[128,1536]{1,0:T(8,128)(2,1)S(1)}, u32[]{:S(2)}, u32[]{:S(2)}) collective-permute-start(bf16[128,1536]{1,0:T(8,128)(2,1)S(1)} %get-tuple-element.37.refs_5_), channel_id=1, source_target_pairs={{0,8},{2,10},{4,12},{6,14},{8,0},{10,2},{12,4},{14,6},{16,24},{18,... | collective-permute-start | bytes 1179656 | tf_op jit(solution)/shard_map/ppermute | solution.py:381
  5.1 20.4 %collective-permute-start.4 = (bf16[128,1536]{1,0:T(8,128)(2,1)S(1)}, bf16[128,1536]{1,0:T(8,128)(2,1)S(1)}, u32[]{:S(2)}, u32[]{:S(2)}) collective-permute-start(bf16[128,1536]{1,0:T(8,128)(2,1)S(1)} %get-tuple-element.37.refs_5_), channel_id=1, source_target_pairs={{0,4},{2,6},{4,0},{6,2},{8,12},{10,14},{12,8},{14,10},{16,20},{18,... | collective-permute-start | bytes 1179656 | tf_op jit(solution)/shard_map/ppermute | solution.py:381
  6.6 18.9 %collective-permute-start.3 = (bf16[128,1536]{1,0:T(8,128)(2,1)S(1)}, bf16[128,1536]{1,0:T(8,128)(2,1)S(1)}, u32[]{:S(2)}, u32[]{:S(2)}) collective-permute-start(bf16[128,1536]{1,0:T(8,128)(2,1)S(1)} %get-tuple-element.37.refs_5_), channel_id=1, source_target_pairs={{0,2},{2,0},{4,6},{6,4},{8,10},{10,8},{12,14},{14,12},{16,18},{18,... | collective-permute-start | bytes 1179656 | tf_op jit(solution)/shard_map/ppermute | solution.py:381
  8.1 9.0 %collective-permute-start = (bf16[16,512]{1,0:T(8,128)(2,1)S(1)}, bf16[16,512]{1,0:T(8,128)(2,1)S(1)}, u32[]{:S(2)}, u32[]{:S(2)}) collective-permute-start(bf16[16,512]{1,0:T(8,128)(2,1)S(1)} %get-tuple-element.34), channel_id=1, source_target_pairs={{0,14},{2,12},{4,10},{6,8},{8,6},{10,4},{12,2},{14,0},{16,30},{18,... | collective-permute-start | bytes 49160 | tf_op jit(solution)/shard_map/ppermute | solution.py:381
  8.1 12.6 %collective-permute-start.1 = (bf16[16,512]{1,0:T(8,128)(2,1)S(1)}, bf16[16,512]{1,0:T(8,128)(2,1)S(1)}, u32[]{:S(2)}, u32[]{:S(2)}) collective-permute-start(bf16[16,512]{1,0:T(8,128)(2,1)S(1)} %get-tuple-element.35), channel_id=1, source_target_pairs={{0,16},{2,18},{4,20},{6,22},{8,24},{10,26},{12,28},{14,30},{16,0},... | collective-permute-start | bytes 49160 | tf_op jit(solution)/shard_map/ppermute | solution.py:381
  17.0 7.6 %collective-permute-start.2 = (bf16[16,512]{1,0:T(8,128)(2,1)S(1)}, bf16[16,512]{1,0:T(8,128)(2,1)S(1)}, u32[]{:S(2)}, u32[]{:S(2)}) collective-permute-start(bf16[16,512]{1,0:T(8,128)(2,1)S(1)} %get-tuple-element.36), channel_id=1, source_target_pairs={{0,30},{2,28},{4,26},{6,24},{8,22},{10,20},{12,18},{14,16},{16,14}... | collective-permute-start | bytes 49160 | tf_op jit(solution)/shard_map/ppermute | solution.py:381
  20.7 20.1 %collective-permute-start.13 = (bf16[512,128]{1,0:T(8,128)(2,1)S(1)}, bf16[512,128]{1,0:T(8,128)(2,1)S(1)}, u32[]{:S(2)}, u32[]{:S(2)}) collective-permute-start(bf16[512,128]{1,0:T(8,128)(2,1)S(1)} %copy-done.6), channel_id=1, source_target_pairs={{0,16},{2,18},{4,20},{6,22},{8,24},{10,26},{12,28},{14,30},{16,0},... | collective-permute-start | bytes 393224 | tf_op jit(solution)/shard_map/ppermute | solution.py:381
  24.6 16.8 %collective-permute-start.12 = (bf16[512,128]{1,0:T(8,128)(2,1)S(1)}, bf16[512,128]{1,0:T(8,128)(2,1)S(1)}, u32[]{:S(2)}, u32[]{:S(2)}) collective-permute-start(bf16[512,128]{1,0:T(8,128)(2,1)S(1)} %copy-done.6), channel_id=1, source_target_pairs={{0,8},{2,10},{4,12},{6,14},{8,0},{10,2},{12,4},{14,6},{16,24},{18,... | collective-permute-start | bytes 393224 | tf_op jit(solution)/shard_map/ppermute | solution.py:381
  25.9 6.8 %collective-permute-start.6 = (bf16[16,1536]{1,0:T(8,128)(2,1)S(1)}, bf16[16,1536]{1,0:T(8,128)(2,1)S(1)}, u32[]{:S(2)}, u32[]{:S(2)}) collective-permute-start(bf16[16,1536]{1,0:T(8,128)(2,1)S(1)} %get-tuple-element.39), channel_id=1, source_target_pairs={{0,14},{2,12},{4,10},{6,8},{8,6},{10,4},{12,2},{14,0},{16,30},{18,... | collective-permute-start | bytes 147464 | tf_op jit(solution)/shard_map/ppermute | solution.py:381
  26.9 8.3 %collective-permute-start.7 = (bf16[16,1536]{1,0:T(8,128)(2,1)S(1)}, bf16[16,1536]{1,0:T(8,128)(2,1)S(1)}, u32[]{:S(2)}, u32[]{:S(2)}) collective-permute-start(bf16[16,1536]{1,0:T(8,128)(2,1)S(1)} %get-tuple-element.40), channel_id=1, source_target_pairs={{0,16},{2,18},{4,20},{6,22},{8,24},{10,26},{12,28},{14,30},{16,0},... | collective-permute-start | bytes 147464 | tf_op jit(solution)/shard_map/ppermute | solution.py:381
  29.1 7.8 %copy-start.3 = (f32[16,4,128,128]{3,2,1,0:T(8,128)S(1)}, f32[16,4,128,128]{3,2,1,0:T(8,128)}, u32[]{:S(2)}) copy-start(f32[16,4,128,128]{3,2,1,0:T(8,128)} %state_ref.1) | copy-start | bytes 12582916
  29.1 7.8 %copy-start.7 = (bf16[16,2048]{1,0:T(8,128)(2,1)S(1)}, bf16[16,2048]{1,0:T(8,128)(2,1)}, u32[]{:S(2)}) copy-start(bf16[16,2048]{1,0:T(8,128)(2,1)} %refs_4_.2) | copy-start | bytes 196612
  29.1 7.8 %copy-start.9 = (f32[512]{0:T(512)S(1)}, f32[512]{0:T(512)}, u32[]{:S(2)}) copy-start(f32[512]{0:T(512)} %param.20) | copy-start | bytes 6148
  29.1 7.8 %copy-start.10 = (f32[512]{0:T(512)S(1)}, f32[512]{0:T(512)}, u32[]{:S(2)}) copy-start(f32[512]{0:T(512)} %param.21) | copy-start | bytes 6148
  29.2 7.8 %collective-permute-start.8 = (bf16[16,1536]{1,0:T(8,128)(2,1)S(1)}, bf16[16,1536]{1,0:T(8,128)(2,1)S(1)}, u32[]{:S(2)}, u32[]{:S(2)}) collective-permute-start(bf16[16,1536]{1,0:T(8,128)(2,1)S(1)} %get-tuple-element.41), channel_id=1, source_target_pairs={{0,30},{2,28},{4,26},{6,24},{8,22},{10,20},{12,18},{14,16},{16,14}... | collective-permute-start | bytes 147464 | tf_op jit(solution)/shard_map/ppermute | solution.py:381
  32.7 8.7 %collective-permute-start.14 = (bf16[512,128]{1,0:T(8,128)(2,1)S(1)}, bf16[512,128]{1,0:T(8,128)(2,1)S(1)}, u32[]{:S(2)}, u32[]{:S(2)}) collective-permute-start(bf16[512,128]{1,0:T(8,128)(2,1)S(1)} %copy-done.6), channel_id=1, source_target_pairs={{0,24},{2,26},{4,28},{6,30},{8,16},{10,18},{12,20},{14,22},{16,8},... | collective-permute-start | bytes 393224 | tf_op jit(solution)/shard_map/ppermute | solution.py:381
  37.9 3.9 %collective-permute-start.9 = (bf16[16,896]{1,0:T(8,128)(2,1)S(1)}, bf16[16,896]{1,0:T(8,128)(2,1)S(1)}, u32[]{:S(2)}, u32[]{:S(2)}) collective-permute-start(bf16[16,896]{1,0:T(8,128)(2,1)S(1)} %get-tuple-element.44), channel_id=1, source_target_pairs={{0,2},{2,0},{4,6},{6,4},{8,10},{10,8},{12,14},{14,12},{16,18},{18,... | collective-permute-start | bytes 86024 | tf_op jit(solution)/shard_map/ppermute | solution.py:381
  39.4 3.9 %collective-permute-start.10 = (bf16[16,896]{1,0:T(8,128)(2,1)S(1)}, bf16[16,896]{1,0:T(8,128)(2,1)S(1)}, u32[]{:S(2)}, u32[]{:S(2)}) collective-permute-start(bf16[16,896]{1,0:T(8,128)(2,1)S(1)} %get-tuple-element.45), channel_id=1, source_target_pairs={{0,4},{2,6},{4,0},{6,2},{8,12},{10,14},{12,8},{14,10},{16,20},{18,... | collective-permute-start | bytes 86024 | tf_op jit(solution)/shard_map/ppermute | solution.py:381
  40.9 4.8 %collective-permute-start.11 = (bf16[16,896]{1,0:T(8,128)(2,1)S(1)}, bf16[16,896]{1,0:T(8,128)(2,1)S(1)}, u32[]{:S(2)}, u32[]{:S(2)}) collective-permute-start(bf16[16,896]{1,0:T(8,128)(2,1)S(1)} %get-tuple-element.46), channel_id=1, source_target_pairs={{0,6},{2,4},{4,2},{6,0},{8,14},{10,12},{12,10},{14,8},{16,22},{18,... | collective-permute-start | bytes 86024 | tf_op jit(solution)/shard_map/ppermute | solution.py:381
  45.9 1.3 %collective-permute-start.15 = (bf16[64,256]{1,0:T(8,128)(2,1)S(1)}, bf16[64,256]{1,0:T(8,128)(2,1)S(1)}, u32[]{:S(2)}, u32[]{:S(2)}) collective-permute-start(bf16[64,256]{1,0:T(8,128)(2,1)S(1)} %get-tuple-element.48), channel_id=1, source_target_pairs={{0,1},{1,0},{2,3},{3,2},{4,5},{5,4},{6,7},{7,6},{8,9},{9,8},{10,11... | collective-permute-start | bytes 98312 | tf_op jit(solution)/shard_map/ppermute | solution.py:384
  47.1 12.7 %copy-start = (bf16[1,2048,1024]{2,1,0:T(8,128)(2,1)S(1)}, bf16[1,2048,1024]{2,1,0:T(8,128)(2,1)}, u32[]{:S(2)}) copy-start(bf16[1,2048,1024]{2,1,0:T(8,128)(2,1)} %gate_ref.3) | copy-start | bytes 12582916
  47.1 12.7 %copy-start.1 = (bf16[1,2048,1024]{2,1,0:T(8,128)(2,1)S(1)}, bf16[1,2048,1024]{2,1,0:T(8,128)(2,1)}, u32[]{:S(2)}) copy-start(bf16[1,2048,1024]{2,1,0:T(8,128)(2,1)} %up_ref.3) | copy-start | bytes 12582916
  47.1 12.7 %copy-start.5 = (f32[2048]{0:T(1024)S(1)}, f32[2048]{0:T(1024)}, u32[]{:S(2)}) copy-start(f32[2048]{0:T(1024)} %param.24) | copy-start | bytes 24580
  59.8 1.4 %collective-permute-start.16 = (bf16[16,24,256]{2,1,0:T(8,128)(2,1)S(1)}, bf16[16,24,256]{2,1,0:T(8,128)(2,1)S(1)}, u32[]{:S(2)}, u32[]{:S(2)}) collective-permute-start(bf16[16,24,256]{2,1,0:T(8,128)(2,1)S(1)} %all_to_all.10.mine_ref), channel_id=1, source_target_pairs={{0,1},{1,0},{2,3},{3,2},{4,5},{5,4},{6,7},{7,6},{8,9},{9,8},{10,11... | collective-permute-start | bytes 589832 | tf_op jit(solution)/shard_map/ppermute | solution.py:384
  59.8 2.2 %copy-start.2 = (bf16[1,1024,2048]{2,1,0:T(8,128)(2,1)S(1)}, bf16[1,1024,2048]{2,1,0:T(8,128)(2,1)}, u32[]{:S(2)}) copy-start(bf16[1,1024,2048]{2,1,0:T(8,128)(2,1)} %down_ref.3) | copy-start | bytes 12582916
  63.8 1.6 %collective-permute-start.17 = (bf16[384,256]{1,0:T(8,128)(2,1)S(1)}, bf16[384,256]{1,0:T(8,128)(2,1)S(1)}, u32[]{:S(2)}, u32[]{:S(2)}) collective-permute-start(bf16[384,256]{1,0:T(8,128)(2,1)S(1)} %get-tuple-element.56), channel_id=1, source_target_pairs={{0,1},{1,0},{2,3},{3,2},{4,5},{5,4},{6,7},{7,6},{8,9},{9,8},{10,11... | collective-permute-start | bytes 589832 | tf_op jit(solution)/shard_map/ppermute | solution.py:384
  66.1 12.5 %all-to-all-start.1 = ((bf16[16,24,256]{2,1,0:T(8,128)(2,1)}), bf16[16,24,256]{2,1,0:T(8,128)(2,1)S(1)}, u32[]{:S(2)}, u32[]{:S(2)}) async-start(bf16[16,24,256]{2,1,0:T(8,128)(2,1)} %bitcast.4), calls=%async_computation.1 | async-start | bytes 393216 | tf_op jit(solution)/shard_map/all_to_all | solution.py:491
  69.6 8.1 %collective-permute-start.18 = (bf16[16,256]{1,0:T(8,128)(2,1)S(1)}, bf16[16,256]{1,0:T(8,128)(2,1)S(1)}, u32[]{:S(2)}, u32[]{:S(2)}) collective-permute-start(bf16[16,256]{1,0:T(8,128)(2,1)S(1)} %get-tuple-element.59), channel_id=1, source_target_pairs={{0,2},{2,0},{4,6},{6,4},{8,10},{10,8},{12,14},{14,12},{16,18},{18,... | collective-permute-start | bytes 24584 | tf_op jit(solution)/shard_map/ppermute | solution.py:381
  71.4 6.3 %collective-permute-start.19 = (bf16[16,256]{1,0:T(8,128)(2,1)S(1)}, bf16[16,256]{1,0:T(8,128)(2,1)S(1)}, u32[]{:S(2)}, u32[]{:S(2)}) collective-permute-start(bf16[16,256]{1,0:T(8,128)(2,1)S(1)} %get-tuple-element.60), channel_id=1, source_target_pairs={{0,4},{2,6},{4,0},{6,2},{8,12},{10,14},{12,8},{14,10},{16,20},{18,... | collective-permute-start | bytes 24584 | tf_op jit(solution)/shard_map/ppermute | solution.py:381
  72.9 4.9 %collective-permute-start.20 = (bf16[16,256]{1,0:T(8,128)(2,1)S(1)}, bf16[16,256]{1,0:T(8,128)(2,1)S(1)}, u32[]{:S(2)}, u32[]{:S(2)}) collective-permute-start(bf16[16,256]{1,0:T(8,128)(2,1)S(1)} %get-tuple-element.61), channel_id=1, source_target_pairs={{0,6},{2,4},{4,2},{6,0},{8,14},{10,12},{12,10},{14,8},{16,22},{18,... | collective-permute-start | bytes 24584 | tf_op jit(solution)/shard_map/ppermute | solution.py:381
  73.2 2.2 %copy-start.4 = (f32[16,4,128,128]{3,2,1,0:T(8,128)S(1)}, f32[16,4,128,128]{3,2,1,0:T(8,128)}, u32[]{:S(2)}) copy-start(f32[16,4,128,128]{3,2,1,0:T(8,128)} %state_ref.1) | copy-start | bytes 12582916
